TPU v7x, 32 devices: a whole 2x2x4 slice. The times are simulated.
32 devices in a mesh: sp: 8 (over z, x), tp: 4 (over y, core).
Axes of the slice: x: 2, y: 2, z: 4, core: 2. Of those that a mesh axis runs over, the one named last changes fastest.
Arguments:
- latent: bfloat16 [2, 4096, 2048], P(None, ('sp', 'tp')), may hold values from -6 to 6
- context: bfloat16 [2, 512, 2048], P(None, 'sp'), may hold values from -6 to 6
- cond: bfloat16 [2, 2048], replicated, may hold values from -6 to 6
- ctx_cond: bfloat16 [2048], replicated, may hold values from -6 to 6
- w_shift: bfloat16 [2048, 2048], P('sp', 'tp'), may hold values from -0.125 to 0.125
- w_scale: bfloat16 [2048, 2048], P('sp', 'tp'), may hold values from -0.125 to 0.125
- w_gate: bfloat16 [2048, 2048], P('sp', 'tp'), may hold values from -0.125 to 0.125
- norm_gain: float32 [2048], replicated, may hold values from 0.1 to 1.9
- w_query: bfloat16 [2048, 2048], P(None, 'tp'), may hold values from -1.08275726 to 1.08275726
- w_key: bfloat16 [2048, 2048], P(None, 'tp'), may hold values from -0.090598056 to 0.090598056
- w_value: bfloat16 [2048, 2048], P(None, 'tp'), may hold values from -0.125 to 0.125
- w_out: bfloat16 [2048, 2048], P('tp'), may hold values from -1.5 to 1.5
- rel_bias: float32 [32, 15, 31], P('tp'), may hold values from -4 to 4
- ctx_bias: float32 [32], P('tp'), may hold values from -3.5 to -2
Outputs:
- mixed: bfloat16 [2, 4096, 2048], P(None, ('sp', 'tp'))
All inputs are finite; a program needn't handle non-finite values.
Results may differ from a plain program's by a relative error of at most 0.0154.
Values may be sent and summed in bfloat16 or wider, within the bound.
A program may use at most 128 MiB of HBM per device.

v0:
```python
import jax
import jax.numpy as jnp
from jax import lax
from jax.sharding import PartitionSpec as P

HEAD_DIM = 64
GRID_W = 64
WIN_ROWS = 8
WIN_COLS = 16


EPSILON = 1e-06


def extended(shard, sides, width):
    for axis, dim in sides:
        size, length = (lax.axis_size(axis), shard.shape[dim])
        up = [(i, (i + 1) % size) for i in range(size - 1)]
        down = [(j, i) for i, j in up]
        last = lax.slice_in_dim(shard, length - width, length, axis=dim)
        first = lax.slice_in_dim(shard, 0, width, axis=dim)
        before = lax.ppermute(last, axis, up)
        after = lax.ppermute(first, axis, down)
        shard = jnp.concatenate([before, shard, after], axis=dim)
    return shard


def silu_rows(values):
    return jax.nn.silu(values.astype(jnp.float32)).astype(jnp.bfloat16)


def modulate_rows(rows, gain, shift, scale):
    floats = rows.astype(jnp.float32)
    inverse = lax.rsqrt(jnp.mean(floats * floats, axis=-1, keepdims=True) + EPSILON)
    return (floats * inverse * gain * (1.0 + scale) + shift).astype(jnp.bfloat16)


def on_device(
    latent,
    context,
    cond,
    ctx_cond,
    w_shift,
    w_scale,
    w_gate,
    norm_gain,
    w_query,
    w_key,
    w_value,
    w_out,
    rel_bias,
    ctx_bias,
):
    samples = latent.shape[0]
    rows_sp = w_shift.shape[0]
    local_cols = w_shift.shape[1]
    sp_index = lax.axis_index("sp")
    ada = silu_rows(jnp.concatenate([cond, ctx_cond[None, :]], axis=0))
    ada_rows = lax.dynamic_slice_in_dim(ada, sp_index * rows_sp, rows_sp, 1)
    partial_value = jnp.stack(
        [
            jnp.dot(ada_rows, weight, preferred_element_type=jnp.float32)
            for weight in (w_shift, w_scale, w_gate)
        ]
    )
    summed = lax.psum(partial_value, "sp")
    modulation = lax.all_gather(summed, "tp", axis=2, tiled=True)
    hidden = modulate_rows(
        latent, norm_gain, modulation[0, :samples, None, :], modulation[1, :samples, None, :]
    )
    w_triple = jnp.concatenate([w_query, w_key, w_value], axis=1)
    triple = jnp.dot(
        lax.all_gather(hidden, "tp", axis=1, tiled=True),
        w_triple,
        preferred_element_type=jnp.float32,
    ).astype(jnp.bfloat16)
    ctx_hidden = modulate_rows(context, norm_gain, modulation[0, samples], modulation[1, samples])
    w_pair = jnp.concatenate([w_key, w_value], axis=1)
    own_pair = jnp.dot(ctx_hidden, w_pair, preferred_element_type=jnp.float32).astype(jnp.bfloat16)
    ctx_pair = lax.all_gather(own_pair, "sp", axis=1, tiled=True)
    heads = local_cols // HEAD_DIM
    tokens_sp = triple.shape[1]
    rows_dev = tokens_sp // GRID_W
    rows_all = rows_dev * lax.axis_size("sp")
    blocks = GRID_W // WIN_COLS
    span = 2 * WIN_COLS
    reach = WIN_ROWS // 2
    padded_count = rows_dev + 2 * reach
    query = triple[..., :local_cols].reshape(samples, rows_dev, GRID_W, local_cols)
    pair = triple[..., local_cols:].reshape(samples, rows_dev, GRID_W, 2 * local_cols)
    padded_pair = extended(pair, (("sp", 1),), reach)
    global_row = sp_index * rows_dev + jnp.arange(rows_dev, dtype=jnp.int32)
    start_row = jnp.clip(global_row - reach, 0, rows_all - WIN_ROWS)
    key_row = sp_index * rows_dev - reach + jnp.arange(padded_count, dtype=jnp.int32)
    row_inside = (key_row[None, :] >= start_row[:, None]) & (
        key_row[None, :] < start_row[:, None] + WIN_ROWS
    )
    row_offset = key_row[None, :] - global_row[:, None] + WIN_ROWS - 1
    row_onehot = (
        row_offset[:, :, None] == jnp.arange(2 * WIN_ROWS - 1, dtype=jnp.int32)[None, None, :]
    ).astype(jnp.float32)
    ctx_count = ctx_pair.shape[1]
    ctx_view = ctx_pair.reshape(samples, ctx_count, 2, heads, HEAD_DIM)
    factor = HEAD_DIM ** (-0.5)
    queries_block = rows_dev * WIN_COLS
    keys_block = padded_count * span
    results = []
    for block in range(blocks):
        first = min(max(WIN_COLS * block - WIN_COLS // 2, 0), GRID_W - span)
        query_col = WIN_COLS * block + jnp.arange(WIN_COLS, dtype=jnp.int32)
        key_col = first + jnp.arange(span, dtype=jnp.int32)
        col_start = jnp.clip(query_col - WIN_COLS // 2, 0, GRID_W - WIN_COLS)
        col_inside = (key_col[None, :] >= col_start[:, None]) & (
            key_col[None, :] < col_start[:, None] + WIN_COLS
        )
        col_onehot = (
            key_col[None, :, None] - query_col[:, None, None] + WIN_COLS - 1
            == jnp.arange(2 * WIN_COLS - 1, dtype=jnp.int32)[None, None, :]
        ).astype(jnp.float32)
        bias = jnp.einsum(
            "rpa,hac,qkc->hrqpk", row_onehot, rel_bias, col_onehot, precision=lax.Precision.HIGHEST
        )
        bias = bias.reshape(heads, queries_block, keys_block)
        inside = (row_inside[:, None, :, None] & col_inside[None, :, None, :]).reshape(
            queries_block, keys_block
        )
        block_query = query[:, :, WIN_COLS * block : WIN_COLS * (block + 1)].reshape(
            samples, queries_block, heads, HEAD_DIM
        )
        block_pair = padded_pair[:, :, first : first + span].reshape(
            samples, keys_block, 2, heads, HEAD_DIM
        )
        near = (
            jnp.einsum(
                "snhd,skhd->shnk",
                block_query,
                block_pair[:, :, 0],
                preferred_element_type=jnp.float32,
            )
            * factor
            + bias[None]
        )
        near = jnp.where(inside[None, None], near, -jnp.inf)
        far = (
            jnp.einsum(
                "snhd,schd->shnc",
                block_query,
                ctx_view[:, :, 0],
                preferred_element_type=jnp.float32,
            )
            * factor
            + ctx_bias[None, :, None, None]
        )
        top = jnp.maximum(jnp.max(near, axis=-1), jnp.max(far, axis=-1))[..., None]
        near_exp = jnp.exp(near - top)
        far_exp = jnp.exp(far - top)
        total = jnp.sum(near_exp, axis=-1, keepdims=True) + jnp.sum(far_exp, axis=-1, keepdims=True)
        near_weight = (near_exp / total).astype(jnp.bfloat16)
        far_weight = (far_exp / total).astype(jnp.bfloat16)
        mixed_near = jnp.einsum(
            "shnk,skhd->snhd", near_weight, block_pair[:, :, 1], preferred_element_type=jnp.float32
        )
        mixed_far = jnp.einsum(
            "shnc,schd->snhd", far_weight, ctx_view[:, :, 1], preferred_element_type=jnp.float32
        )
        results.append(
            (mixed_near + mixed_far)
            .astype(jnp.bfloat16)
            .reshape(samples, rows_dev, WIN_COLS, local_cols)
        )
    attended = jnp.stack(results, axis=2).reshape(samples, tokens_sp, local_cols).transpose(1, 0, 2)
    update = lax.psum_scatter(
        jnp.einsum("tsc,cd->tsd", attended, w_out, preferred_element_type=jnp.float32).astype(
            jnp.bfloat16
        ),
        "tp",
        scatter_dimension=0,
        tiled=True,
    ).astype(jnp.float32)
    gate = modulation[2, :samples, None, :]
    result = latent.astype(jnp.float32) + gate * update.transpose(1, 0, 2)
    return result.astype(jnp.bfloat16)


def solution(mesh):
    return jax.shard_map(
        on_device,
        mesh=mesh,
        in_specs=(
            P(None, ("sp", "tp"), None),
            P(None, "sp", None),
            P(),
            P(),
            P("sp", "tp"),
            P("sp", "tp"),
            P("sp", "tp"),
            P(),
            P(None, "tp"),
            P(None, "tp"),
            P(None, "tp"),
            P("tp", None),
            P("tp", None, None),
            P("tp"),
        ),
        out_specs=P(None, ("sp", "tp"), None),
        check_vma=False,
    )
```

profile of v0, /device:TPU:0, one launch (start us, length us, event | category | flops | bytes accessed | tf_op | source)
XLA Modules:
  0.0 414.4 jit_solution(15274392591690671827)
XLA Ops:
  11.4 38.9 %psum.7 = f32[3,3,512]{2,1,0:T(4,128)S(1)} all-reduce(f32[3,3,512]{2,1,0:T(4,128)S(1)} %pad_maximum_fusion.2), channel_id=1, replica_groups=mesh['sp'=8,'tp'=4] {'sp'}, use_global_device_ids=true, to_apply=%region_0.1 | all-reduce | flops 4608 | bytes 36864 | tf_op jit(solution)/shard_map/psum | solution.py:66
  50.3 5.3 %all_gather.9 = f32[3,3,2048]{2,1,0:T(4,128)S(1)} all-gather(f32[3,3,512]{2,1,0:T(4,128)S(1)} %psum.7), channel_id=1, replica_groups=mesh['sp'=8,'tp'=4] {'tp'}, dimensions={2}, use_global_device_ids=true | all-gather | bytes 92160 | tf_op jit(solution)/shard_map/all_gather | solution.py:67
  69.5 4.3 %copy.25 = f32[8,8,16,16,32]{4,3,2,1,0:T(8,128)} copy(f32[8,8,16,16,32]{4,3,1,0,2:T(8,128)S(1)} %convolution_bitcast_fusion.3) | data formatting | bytes 4194304 | tf_op jit(solution)/shard_map/rpa,hac,qkc->hrqpk/transpose | solution.py:120
  73.8 7.5 %add.449 = f32[8,128,512]{2,1,0:T(8,128)} reshape(f32[8,8,16,16,32]{4,3,2,1,0:T(8,128)} %copy.25) | data formatting | bytes 4194304 | tf_op jit(solution)/shard_map/add | solution.py:134
  86.2 4.3 %copy.46 = f32[8,8,16,16,32]{4,3,2,1,0:T(8,128)} copy(f32[8,8,16,16,32]{4,3,1,0,2:T(8,128)S(1)} %convolution_bitcast_fusion) | data formatting | bytes 4194304 | tf_op jit(solution)/shard_map/rpa,hac,qkc->hrqpk/transpose | solution.py:120
  90.5 7.6 %add.487 = f32[8,128,512]{2,1,0:T(8,128)} reshape(f32[8,8,16,16,32]{4,3,2,1,0:T(8,128)} %copy.46) | data formatting | bytes 4194304 | tf_op jit(solution)/shard_map/add | solution.py:134
  107.8 7.5 %add.477 = f32[8,128,512]{2,1,0:T(8,128)} reshape(f32[8,8,16,16,32]{4,3,2,1,0:T(8,128)} %copy.40) | data formatting | bytes 4194304 | tf_op jit(solution)/shard_map/add | solution.py:134
  120.9 4.3 %copy.34 = f32[8,8,16,16,32]{4,3,2,1,0:T(8,128)} copy(f32[8,8,16,16,32]{4,3,1,0,2:T(8,128)S(1)} %convolution_bitcast_fusion.2) | data formatting | bytes 4194304 | tf_op jit(solution)/shard_map/rpa,hac,qkc->hrqpk/transpose | solution.py:120
  125.1 7.7 %add.467 = f32[8,128,512]{2,1,0:T(8,128)} reshape(f32[8,8,16,16,32]{4,3,2,1,0:T(8,128)} %copy.34) | data formatting | bytes 4194304 | tf_op jit(solution)/shard_map/add | solution.py:134
  136.8 5.2 %all-gather.3.cloned.1.call-done = bf16[2,512,2048]{2,1,0:T(8,128)(2,1)} async-done(((bf16[2,128,2048]{2,1,0:T(8,128)(2,1)}), bf16[2,512,2048]{2,1,0:T(8,128)(2,1)}) %all-gather.3.cloned.1.call-update) | async-done | bytes 4194320 | tf_op jit(solution)/shard_map/all_gather | solution.py:73
  141.9 10.7 %fusion.6 = bf16[2,512,1536]{2,1,0:T(8,128)(2,1)S(1)} fusion(bf16[2,512,2048]{2,1,0:T(8,128)(2,1)} %all-gather.3.cloned.1.call-done, bf16[2048,512]{1,0:T(8,128)(2,1)} %param.24, bf16[2048,512]{1,0:T(8,128)(2,1)} %param.23, bf16[2048,512]{1,0:T(8,128)(2,1)} %param.22), kind=kOutput, calls=%fused_computation.33 | convolution fusion | flops 6462898176 | bytes 13631488 | tf_op jit(solution)/shard_map/dot_general | solution.py:72
  154.7 4.3 %collective-permute-start = (bf16[2,4,64,1024]{3,2,1,0:T(8,128)(2,1)}, bf16[2,4,64,1024]{3,2,1,0:T(8,128)(2,1)}, u32[]{:S(2)}, u32[]{:S(2)}) collective-permute-start(bf16[2,4,64,1024]{3,2,1,0:T(8,128)(2,1)} %get-tuple-element.32), channel_id=1, source_target_pairs={{0,4},{4,8},{8,12},{12,16},{16,20},{20,24},{24,28},{1,5},{5,9},{9,... | collective-permute-start | bytes 3145736 | tf_op jit(solution)/shard_map/ppermute | solution.py:22
  177.2 26.4 %collective-permute-done = bf16[2,4,64,1024]{3,2,1,0:T(8,128)(2,1)} collective-permute-done((bf16[2,4,64,1024]{3,2,1,0:T(8,128)(2,1)}, bf16[2,4,64,1024]{3,2,1,0:T(8,128)(2,1)}, u32[]{:S(2)}, u32[]{:S(2)}) %collective-permute-start) | collective-permute-done | bytes 1048608 | tf_op jit(solution)/shard_map/ppermute | solution.py:22
  209.3 6.4 %reshape.658 = bf16[2,512,2,8,64]{4,3,2,1,0:T(8,128)(2,1)} reshape(bf16[2,16,32,1024]{3,2,1,0:T(8,128)(2,1)} %get-tuple-element.31) | data formatting | bytes 4194304 | tf_op jit(solution)/shard_map/reshape | solution.py:130
  215.7 4.5 %fusion.122 = (bf16[2,512,1,8,64]{4,3,2,1,0:T(8,128)(2,1)}, bf16[2,512,1,8,64]{4,3,2,1,0:T(8,128)(2,1)}) fusion(bf16[2,512,2,8,64]{4,3,2,1,0:T(8,128)(2,1)} %reshape.658), kind=kLoop, calls=%fused_computation.204 | loop fusion | bytes 4194304 | tf_op jit(solution)/shard_map/slice | solution.py:161
  226.3 9.0 %fusion.15 = (f32[2,8,128]{2,1,0:T(8,128)S(1)}, f32[2,8,128]{2,1,0:T(8,128)S(1)}, f32[2,8,128]{2,1,0:T(8,128)S(1)}, f32[2,8,128]{2,1,0:T(8,128)}, f32[2,8,128]{2,1,0:T(8,128)}, /*index=5*/f32[2,8,128,512]{3,2,1,0:T(8,128)}) fusion(f32[2,8,128,512]{3,2,1,0:T(8,128)} %get-tuple-element.52, f32[2,8,128]{2,1,0:T(8,128)S(1)} %max.48, f32[8]{0:T(128)S(1)} %copy-done.39, ...), kind=kOutput, calls=%fused_computation.47 | convolution fusion | flops 153081856 | bytes 24494112 | tf_op jit(solution)/shard_map/snhd,schd->shnc/dot_general | solution.py:145
  240.2 5.2 %fusion.50 = bf16[2,128,8,64]{1,3,2,0:T(8,128)(2,1)} fusion(f32[2,8,64,128]{3,2,1,0:T(8,128)} %fusion.30, f32[2,8,128,512]{3,2,1,0:T(8,128)} %copy-done.17, f32[2,8,128]{2,1,0:T(8,128)} %copy-done.42, f32[2,8,128]{2,1,0:T(8,128)} %copy-done.36, f32[8,128,512]{2,1,0:T(8,128)} %add.449, pred[128,512]{1,0:T(8,128)(4,1)S(1)} %and.115, ...), kind=kOutput, calls=%fused_computation.91 | convolution fusion | flops 140771328 | bytes 8208384 | tf_op jit(solution)/shard_map/shnk,skhd->snhd/dot_general | solution.py:160
  247.7 6.4 %reshape.666 = bf16[2,512,2,8,64]{4,3,2,1,0:T(8,128)(2,1)} reshape(bf16[2,16,32,1024]{3,2,1,0:T(8,128)(2,1)} %get-tuple-element.28) | data formatting | bytes 4194304 | tf_op jit(solution)/shard_map/reshape | solution.py:130
  254.1 4.5 %fusion.125 = (bf16[2,512,1,8,64]{4,3,2,1,0:T(8,128)(2,1)}, bf16[2,512,1,8,64]{4,3,2,1,0:T(8,128)(2,1)}) fusion(bf16[2,512,2,8,64]{4,3,2,1,0:T(8,128)(2,1)} %reshape.666), kind=kLoop, calls=%fused_computation.207 | loop fusion | bytes 4194304 | tf_op jit(solution)/shard_map/slice | solution.py:161
  261.1 6.5 %reshape.664 = bf16[2,512,2,8,64]{4,3,2,1,0:T(8,128)(2,1)} reshape(bf16[2,16,32,1024]{3,2,1,0:T(8,128)(2,1)} %get-tuple-element.29) | data formatting | bytes 4194304 | tf_op jit(solution)/shard_map/reshape | solution.py:130
  267.6 4.5 %fusion.124 = (bf16[2,512,1,8,64]{4,3,2,1,0:T(8,128)(2,1)}, bf16[2,512,1,8,64]{4,3,2,1,0:T(8,128)(2,1)}) fusion(bf16[2,512,2,8,64]{4,3,2,1,0:T(8,128)(2,1)} %reshape.664), kind=kLoop, calls=%fused_computation.206 | loop fusion | bytes 4194304 | tf_op jit(solution)/shard_map/slice | solution.py:161
  275.5 6.4 %reshape.662 = bf16[2,512,2,8,64]{4,3,2,1,0:T(8,128)(2,1)} reshape(bf16[2,16,32,1024]{3,2,1,0:T(8,128)(2,1)} %get-tuple-element.30) | data formatting | bytes 4194304 | tf_op jit(solution)/shard_map/reshape | solution.py:130
  282.0 4.5 %fusion.123 = (bf16[2,512,1,8,64]{4,3,2,1,0:T(8,128)(2,1)}, bf16[2,512,1,8,64]{4,3,2,1,0:T(8,128)(2,1)}) fusion(bf16[2,512,2,8,64]{4,3,2,1,0:T(8,128)(2,1)} %reshape.662), kind=kLoop, calls=%fused_computation.205 | loop fusion | bytes 4194304 | tf_op jit(solution)/shard_map/slice | solution.py:161
  302.0 9.1 %fusion.16 = (f32[2,8,128]{2,1,0:T(8,128)S(1)}, f32[2,8,128]{2,1,0:T(8,128)S(1)}, f32[2,8,128]{2,1,0:T(8,128)S(1)}, f32[2,8,128]{2,1,0:T(8,128)S(1)}, f32[2,8,128]{2,1,0:T(8,128)}, /*index=5*/f32[2,8,128]{2,1,0:T(8,128)}) fusion(f32[2,8,128,512]{3,2,1,0:T(8,128)} %get-tuple-element.53, f32[2,8,128]{2,1,0:T(8,128)S(1)} %max.49, f32[8]{0:T(128)S(1)} %copy-done.40, ...), kind=kLoop, calls=%fused_computation.48 | loop fusion | flops 28299264 | bytes 31727648 | tf_op jit(solution)/shard_map/reduce_sum | solution.py:157
  311.2 4.4 %fusion.31 = f32[2,8,64,128]{3,2,1,0:T(8,128)} fusion(f32[2,8,128,512]{3,2,1,0:T(8,128)} %get-tuple-element.53, f32[2,8,128]{2,1,0:T(8,128)S(1)} %add.471, f32[2,8,128]{2,1,0:T(8,128)S(1)} %max.49, f32[8]{0:T(128)S(1)} %copy-done.40, bf16[2,512,2,8,64]{1,4,3,2,0:T(8,128)(2,1)S(1)} %bitcast.212), kind=kOutput, calls=%fused_computation.66 | convolution fusion | flops 139460608 | bytes 5784064 | tf_op jit(solution)/shard_map/shnc,schd->snhd/dot_general | solution.py:163
  318.4 5.2 %fusion.49 = bf16[2,128,8,64]{1,3,2,0:T(8,128)(2,1)} fusion(f32[2,8,64,128]{3,2,1,0:T(8,128)} %fusion.31, f32[2,8,128,512]{3,2,1,0:T(8,128)} %copy-done.15, f32[2,8,128]{2,1,0:T(8,128)S(1)} %add.471, f32[2,8,128]{2,1,0:T(8,128)S(1)} %max.49, f32[8,128,512]{2,1,0:T(8,128)} %add.467, pred[128,512]{1,0:T(8,128)(4,1)S(1)} %copy-done.30, ...), kind=kOutput, calls=%fused_computation.90 | convolution fusion | flops 140771328 | bytes 8208384 | tf_op jit(solution)/shard_map/shnk,skhd->snhd/dot_general | solution.py:160
  325.8 4.7 %fusion.32 = f32[2,8,64,128]{3,2,1,0:T(8,128)} fusion(f32[2,8,128,512]{3,2,1,0:T(8,128)} %fusion.69, f32[2,8,128]{2,1,0:T(8,128)S(1)} %add.481, f32[2,8,128]{2,1,0:T(8,128)S(1)} %copy-done.35, f32[8]{0:T(128)S(1)} %copy-done.41, bf16[2,512,2,8,64]{1,4,3,2,0:T(8,128)(2,1)} %bitcast.207), kind=kOutput, calls=%fused_computation.67 | convolution fusion | flops 139460608 | bytes 5783584 | tf_op jit(solution)/shard_map/shnc,schd->snhd/dot_general | solution.py:163
  333.0 4.5 %fusion.48 = bf16[2,128,8,64]{1,3,2,0:T(8,128)(2,1)S(1)} fusion(f32[2,8,64,128]{3,2,1,0:T(8,128)} %fusion.32, f32[2,8,128,512]{3,2,1,0:T(8,128)} %copy-done.14, f32[2,8,128]{2,1,0:T(8,128)} %copy-done.43, f32[2,8,128]{2,1,0:T(8,128)S(1)} %copy-done.35, f32[8,128,512]{2,1,0:T(8,128)} %add.477, pred[128,512]{1,0:T(8,128)(4,1)S(1)} %copy-done.28, ...), kind=kOutput, calls=%fused_computation.89 | convolution fusion | flops 140771328 | bytes 8208384 | tf_op jit(solution)/shard_map/shnk,skhd->snhd/dot_general | solution.py:160
  339.6 4.6 %fusion.33 = f32[2,8,64,128]{3,2,1,0:T(8,128)} fusion(f32[2,8,128,512]{3,2,1,0:T(8,128)} %fusion.68, f32[2,8,128]{2,1,0:T(8,128)S(1)} %add.491, f32[2,8,128]{2,1,0:T(8,128)S(1)} %max.51, f32[8]{0:T(128)} %param.27, bf16[2,512,2,8,64]{1,4,3,2,0:T(8,128)(2,1)} %bitcast.208), kind=kOutput, calls=%fused_computation.68 | convolution fusion | flops 139460608 | bytes 5784064 | tf_op jit(solution)/shard_map/shnc,schd->snhd/dot_general | solution.py:163
  346.7 5.2 %fusion.47 = bf16[2,128,8,64]{1,3,2,0:T(8,128)(2,1)} fusion(f32[2,8,64,128]{3,2,1,0:T(8,128)} %fusion.33, f32[2,8,128,512]{3,2,1,0:T(8,128)} %copy-done.13, f32[2,8,128]{2,1,0:T(8,128)S(1)} %add.491, f32[2,8,128]{2,1,0:T(8,128)S(1)} %max.51, f32[8,128,512]{2,1,0:T(8,128)} %add.487, pred[128,512]{1,0:T(8,128)(4,1)S(1)} %and.127, ...), kind=kOutput, calls=%fused_computation.88 | convolution fusion | flops 140771328 | bytes 8208384 | tf_op jit(solution)/shard_map/shnk,skhd->snhd/dot_general | solution.py:160
  354.8 4.3 %convolution_convert_fusion = bf16[512,2,2048]{2,0,1:T(8,128)(2,1)} fusion(bf16[512,2,512]{2,0,1:T(8,128)(2,1)S(1)} %bitcast.220, bf16[512,2048]{1,0:T(8,128)(2,1)S(1)} %copy-done), kind=kOutput, calls=%fused_computation.34 | convolution fusion | flops 2149580800 | bytes 7340032 | tf_op jit(solution)/shard_map/tsc,cd->tsd/dot_general | solution.py:173
  359.1 45.7 %reduce-scatter.2.cloned.1.call-done = bf16[128,2,2048]{2,0,1:T(8,128)(2,1)} async-done(((bf16[512,2,2048]{2,0,1:T(8,128)(2,1)}), bf16[128,2,2048]{2,0,1:T(8,128)(2,1)}) %reduce-scatter.2.cloned.1.call-update) | async-done | bytes 1048592 | tf_op jit(solution)/shard_map/reduce_scatter | solution.py:172
  (198 shorter events, 120.8 us)
Async XLA Ops:
  6.5 348.3 %copy-start = (bf16[512,2048]{1,0:T(8,128)(2,1)S(1)}, bf16[512,2048]{1,0:T(8,128)(2,1)}, u32[]{:S(2)}) copy-start(bf16[512,2048]{1,0:T(8,128)(2,1)} %param.25) | copy-start | bytes 6291460
  6.5 126.3 %all-gather.5.cloned.1.call-start = ((), (), s32[]{:S(2)}) async-start(), calls=%async_computation.2 | async-start | bytes 2359296 | tf_op jit(solution)/shard_map/all_gather | solution.py:80
  56.8 5.0 %copy-start.37 = (f32[2048]{0:T(1024)S(1)}, f32[2048]{0:T(1024)}, u32[]{:S(2)}) copy-start(f32[2048]{0:T(1024)} %param.21) | copy-start | bytes 24580
  60.9 81.1 %all-gather.3.cloned.1.call-start = ((), (), s32[]{:S(2)}) async-start(), calls=%async_computation.1 | async-start | bytes 5242880 | tf_op jit(solution)/shard_map/all_gather | solution.py:73
  63.4 341.5 %reduce-scatter.2.cloned.1.call-start = ((), (), s32[]{:S(2)}) async-start(), calls=%async_computation.3 | async-start | bytes 5242880 | tf_op jit(solution)/shard_map/reduce_scatter | solution.py:172
  152.9 8.3 %copy-start.11 = (bf16[2,512,1024]{2,1,0:T(8,128)(2,1)}, bf16[2,512,1024]{2,1,0:T(8,128)(2,1)S(1)}, u32[]{:S(2)}) copy-start(bf16[2,512,1024]{2,1,0:T(8,128)(2,1)S(1)} %slice.117) | copy-start | bytes 6291460
  154.7 49.0 %collective-permute-start = (bf16[2,4,64,1024]{3,2,1,0:T(8,128)(2,1)}, bf16[2,4,64,1024]{3,2,1,0:T(8,128)(2,1)}, u32[]{:S(2)}, u32[]{:S(2)}) collective-permute-start(bf16[2,4,64,1024]{3,2,1,0:T(8,128)(2,1)} %get-tuple-element.32), channel_id=1, source_target_pairs={{0,4},{4,8},{8,12},{12,16},{16,20},{20,24},{24,28},{1,5},{5,9},{9,... | collective-permute-start | bytes 3145736 | tf_op jit(solution)/shard_map/ppermute | solution.py:22
  159.1 44.6 %collective-permute-start.1 = (bf16[2,4,64,1024]{3,2,1,0:T(8,128)(2,1)}, bf16[2,4,64,1024]{3,2,1,0:T(8,128)(2,1)}, u32[]{:S(2)}, u32[]{:S(2)}) collective-permute-start(bf16[2,4,64,1024]{3,2,1,0:T(8,128)(2,1)} %get-tuple-element.33), channel_id=1, source_target_pairs={{4,0},{8,4},{12,8},{16,12},{20,16},{24,20},{28,24},{5,1},{9,5},{13... | collective-permute-start | bytes 3145736 | tf_op jit(solution)/shard_map/ppermute | solution.py:23
  161.8 12.7 %copy-start.22 = (bf16[2,128,8,64]{1,3,2,0:T(8,128)(2,1)}, bf16[2,128,8,64]{1,3,2,0:T(8,128)(2,1)S(1)}, u32[]{:S(2)}) copy-start(bf16[2,128,8,64]{1,3,2,0:T(8,128)(2,1)S(1)} %copy.24) | copy-start | bytes 786436
  162.5 9.3 %copy-start.23 = (bf16[2,128,8,64]{1,3,2,0:T(8,128)(2,1)}, bf16[2,128,8,64]{1,3,2,0:T(8,128)(2,1)S(1)}, u32[]{:S(2)}) copy-start(bf16[2,128,8,64]{1,3,2,0:T(8,128)(2,1)S(1)} %copy.39) | copy-start | bytes 786436
  164.2 10.4 %copy-start.25 = (bf16[2,128,8,64]{1,3,2,0:T(8,128)(2,1)}, bf16[2,128,8,64]{1,3,2,0:T(8,128)(2,1)S(1)}, u32[]{:S(2)}) copy-start(bf16[2,128,8,64]{1,3,2,0:T(8,128)(2,1)S(1)} %copy.45) | copy-start | bytes 786436
  167.7 6.9 %copy-start.38 = (f32[8]{0:T(128)S(1)}, f32[8]{0:T(128)}, u32[]{:S(2)}) copy-start(f32[8]{0:T(128)} %param.27) | copy-start | bytes 100
  171.8 31.9 %copy-start.12 = (bf16[2,512,1024]{2,1,0:T(8,128)(2,1)S(1)}, bf16[2,512,1024]{2,1,0:T(8,128)(2,1)}, u32[]{:S(2)}) copy-start(bf16[2,512,1024]{2,1,0:T(8,128)(2,1)} %copy-done.11) | copy-start | bytes 6291460
  225.6 9.7 %copy-start.17 = (f32[2,8,128,512]{3,2,1,0:T(8,128)}, f32[2,8,128,512]{3,2,1,0:T(8,128)S(1)}, u32[]{:S(2)}) copy-start(f32[2,8,128,512]{3,2,1,0:T(8,128)S(1)} %get-tuple-element.50) | copy-start | bytes 12582916
  225.6 9.7 %copy-start.36 = (f32[2,8,128]{2,1,0:T(8,128)}, f32[2,8,128]{2,1,0:T(8,128)S(1)}, u32[]{:S(2)}) copy-start(f32[2,8,128]{2,1,0:T(8,128)S(1)} %max.48) | copy-start | bytes 24580
  226.3 9.1 %copy-start.9 = (bf16[2,512,1024]{1,2,0:T(8,128)(2,1)S(1)}, bf16[2,512,1024]{1,2,0:T(8,128)(2,1)}, u32[]{:S(2)}) copy-start(bf16[2,512,1024]{1,2,0:T(8,128)(2,1)} %copy.26) | copy-start | bytes 6291460
  226.3 9.1 %copy-start.16 = (f32[2,8,128,512]{3,2,1,0:T(8,128)S(1)}, f32[2,8,128,512]{3,2,1,0:T(8,128)}, u32[]{:S(2)}) copy-start(f32[2,8,128,512]{3,2,1,0:T(8,128)} %get-tuple-element.52) | copy-start | bytes 12582916
  292.6 5.4 %copy-start.13 = (f32[2,8,128,512]{3,2,1,0:T(8,128)}, f32[2,8,128,512]{3,2,1,0:T(8,128)S(1)}, u32[]{:S(2)}) copy-start(f32[2,8,128,512]{3,2,1,0:T(8,128)S(1)} %get-tuple-element.57) | copy-start | bytes 12582916
  292.8 6.0 %copy-start.3 = (f32[2,8,128,512]{3,2,1,0:T(8,128)S(1)}, f32[2,8,128,512]{3,2,1,0:T(8,128)}, u32[]{:S(2)}) copy-start(f32[2,8,128,512]{3,2,1,0:T(8,128)} %fusion.69) | copy-start | bytes 12582916
  293.9 17.2 %copy-start.14 = (f32[2,8,128,512]{3,2,1,0:T(8,128)}, f32[2,8,128,512]{3,2,1,0:T(8,128)S(1)}, u32[]{:S(2)}) copy-start(f32[2,8,128,512]{3,2,1,0:T(8,128)S(1)} %get-tuple-element.55) | copy-start | bytes 12582916
  294.0 7.5 %copy-start.2 = (f32[2,8,128,512]{3,2,1,0:T(8,128)S(1)}, f32[2,8,128,512]{3,2,1,0:T(8,128)}, u32[]{:S(2)}) copy-start(f32[2,8,128,512]{3,2,1,0:T(8,128)} %fusion.68) | copy-start | bytes 12582916
  294.0 8.1 %copy-start.5 = (f32[8,128,512]{2,1,0:T(8,128)S(1)}, f32[8,128,512]{2,1,0:T(8,128)}, u32[]{:S(2)}) copy-start(f32[8,128,512]{2,1,0:T(8,128)} %add.487) | copy-start | bytes 6291460
  294.0 8.1 %copy-start.40 = (f32[8]{0:T(128)S(1)}, f32[8]{0:T(128)}, u32[]{:S(2)}) copy-start(f32[8]{0:T(128)} %param.27) | copy-start | bytes 100
  296.8 14.3 %copy-start.34 = (f32[2,8,128]{2,1,0:T(8,128)}, f32[2,8,128]{2,1,0:T(8,128)S(1)}, u32[]{:S(2)}) copy-start(f32[2,8,128]{2,1,0:T(8,128)S(1)} %max.50) | copy-start | bytes 24580
  298.0 13.2 %copy-start.15 = (f32[2,8,128,512]{3,2,1,0:T(8,128)}, f32[2,8,128,512]{3,2,1,0:T(8,128)S(1)}, u32[]{:S(2)}) copy-start(f32[2,8,128,512]{3,2,1,0:T(8,128)S(1)} %get-tuple-element.48) | copy-start | bytes 12582916
  302.0 9.1 %copy-start.10 = (bf16[2,512,1024]{1,2,0:T(8,128)(2,1)S(1)}, bf16[2,512,1024]{1,2,0:T(8,128)(2,1)}, u32[]{:S(2)}) copy-start(bf16[2,512,1024]{1,2,0:T(8,128)(2,1)} %copy.26) | copy-start | bytes 6291460
  311.2 7.1 %copy-start.30 = (pred[128,512]{1,0:T(8,128)(4,1)S(1)}, pred[128,512]{1,0:T(8,128)(4,1)}, u32[]{:S(2)}) copy-start(pred[128,512]{1,0:T(8,128)(4,1)} %and.119) | copy-start | bytes 196612
  318.4 7.5 %copy-start.35 = (f32[2,8,128]{2,1,0:T(8,128)S(1)}, f32[2,8,128]{2,1,0:T(8,128)}, u32[]{:S(2)}) copy-start(f32[2,8,128]{2,1,0:T(8,128)} %copy-done.34) | copy-start | bytes 24580
  318.4 7.5 %copy-start.41 = (f32[8]{0:T(128)S(1)}, f32[8]{0:T(128)}, u32[]{:S(2)}) copy-start(f32[8]{0:T(128)} %param.27) | copy-start | bytes 100
  346.7 6.8 %copy-start.27 = (bf16[2,8,1,16,512]{4,3,1,0,2:T(8,128)(2,1)S(1)}, bf16[2,8,1,16,512]{4,3,1,0,2:T(8,128)(2,1)}, u32[]{:S(2)}) copy-start(bf16[2,8,1,16,512]{4,3,1,0,2:T(8,128)(2,1)} %stack_reshape.12) | copy-start | bytes 786436
  359.1 45.7 %copy-start.19 = (bf16[2,128,2048]{2,1,0:T(8,128)(2,1)S(1)}, bf16[2,128,2048]{2,1,0:T(8,128)(2,1)}, u32[]{:S(2)}) copy-start(bf16[2,128,2048]{2,1,0:T(8,128)(2,1)} %param.14) | copy-start | bytes 3145732
  359.1 45.7 %copy-start.31 = (f32[2,2048]{1,0:T(2,128)S(1)}, f32[2,2048]{1,0:T(2,128)}, u32[]{:S(2)}) copy-start(f32[2,2048]{1,0:T(2,128)} %get-tuple-element.38) | copy-start | bytes 49156
  (17 other events, 57.2 us)
Sparse Core Ops, SparseCore 0:
  61.0 46.3 all-gather.4
  108.9 32.9 all-gather.2
  359.3 45.5 reduce-scatter.1
where the time goes:
time: 422 us; the launch traced here: 414 us
  local copies, waits for them, and re-layouts  149 us (35%)
  matrix products  102 us (24%)
  waiting for transfers between devices  77.3 us (18%)
  blocking collectives  44.2 us (10%)
  other arithmetic  21.4 us (5%)
  between operations  14.3 us (3%)
  starting transfers between devices  5.72 us (1%)
    reduce_scatter x1, waiting for transfers between devices, on_device(): lax.psum_scatter(jnp.einsum('tsc,cd->tsd', attended, w_out, preferred_ele...  45.7 us
    psum x1, blocking collectives, on_device(): summed = lax.psum(partial_value, 'sp')  38.9 us
    add x4, local copies, waits for them, and re-layouts, on_device(): jnp.einsum('snhd,skhd->shnk', block_query, block_pair[:, :, 0], preferred...  30.2 us
    unnamed x96, local copies, waits for them, and re-layouts  29.8 us
    ppermute x1, waiting for transfers between devices, extended(): before = lax.ppermute(last, axis, up)  26.4 us
    reshape x4, local copies, waits for them, and re-layouts, on_device(): padded_pair[:, :, first:first + span]  25.8 us
    dot_general x4, matrix products, on_device(): jnp.einsum('shnk,skhd->snhd', near_weight, block_pair[:, :, 1], preferred...  20 us
    dot_general x4, matrix products, on_device(): jnp.einsum('snhd,schd->shnc', block_query, ctx_view[:, :, 0], preferred_e...  18.6 us
  transfers between devices with their start and end apart: 5, of which 3 were waited for; matrix products, arithmetic and copies ran while one was open for 22% of the time, Pallas kernels for 0%

commit v1 on v0

v1 whole, which is shorter than its diff:
```python
import jax
import jax.numpy as jnp
from jax import lax
from jax.experimental import pallas as pl
from jax.experimental.pallas import tpu as pltpu
from jax.sharding import PartitionSpec as P

HEAD_DIM = 64
GRID_W = 64
WIN_ROWS = 8
WIN_COLS = 16


EPSILON = 1e-06


def extended(shard, sides, width):
    for axis, dim in sides:
        size, length = (lax.axis_size(axis), shard.shape[dim])
        up = [(i, (i + 1) % size) for i in range(size - 1)]
        down = [(j, i) for i, j in up]
        last = lax.slice_in_dim(shard, length - width, length, axis=dim)
        first = lax.slice_in_dim(shard, 0, width, axis=dim)
        before = lax.ppermute(last, axis, up)
        after = lax.ppermute(first, axis, down)
        shard = jnp.concatenate([before, shard, after], axis=dim)
    return shard


def silu_rows(values):
    return jax.nn.silu(values.astype(jnp.float32)).astype(jnp.bfloat16)


def modulate_rows(rows, gain, shift, scale):
    floats = rows.astype(jnp.float32)
    inverse = lax.rsqrt(jnp.mean(floats * floats, axis=-1, keepdims=True) + EPSILON)
    return (floats * inverse * gain * (1.0 + scale) + shift).astype(jnp.bfloat16)

LOG2E = 1.4426950408889634


def attention_kernel(bias_ref, far_ref, q_ref, k_ref, v_ref, ck_ref, cv_ref, out_ref, table):
    pair = pl.program_id(0)
    rows_dev = q_ref.shape[1]
    padded = k_ref.shape[1]
    span = 2 * WIN_COLS
    half = WIN_COLS // 2
    reach = WIN_ROWS // 2
    nq, nk = rows_dev * WIN_COLS, padded * span
    lanes = 2 * HEAD_DIM

    @pl.when(pl.program_id(1) == 0)
    def _():
        sp = lax.axis_index("sp")
        rows_all = rows_dev * lax.axis_size("sp")
        at = lax.broadcasted_iota(jnp.int32, (WIN_COLS, nk), 1)
        p = lax.broadcasted_iota(jnp.int32, (WIN_COLS, nk), 0)
        key_row = sp * rows_dev - reach + at // span
        k = at % span
        inner = (k - p >= 0) & (k - p < WIN_COLS)
        edge = (p < half) == (k < WIN_COLS)
        for r in range(rows_dev):
            row = sp * rows_dev + r
            first = jnp.clip(row - reach, 0, rows_all - WIN_ROWS)
            inside = (key_row >= first) & (key_row < first + WIN_ROWS)
            shift = span * (r + reach - WIN_ROWS + 1) - half + 1
            for h in range(2):
                line = jnp.broadcast_to(bias_ref[0, h : h + 1, :], (WIN_COLS, nk))
                line = pltpu.roll(line, shift % nk, 1, stride=1, stride_axis=0) * LOG2E
                at_rows = pl.ds(r * WIN_COLS, WIN_COLS)
                table[h, 0, at_rows, :] = jnp.where(inside & edge, line, -jnp.inf)
                table[h, 1, at_rows, :] = jnp.where(inside & inner, line, -jnp.inf)

    factor = HEAD_DIM ** (-0.5) * LOG2E
    ck = ck_ref[0]
    ctx_count = ck.shape[0]
    cv = jnp.concatenate([cv_ref[0], jnp.ones((ctx_count, lanes), jnp.bfloat16)], axis=1)
    ones = jnp.ones((nk, lanes), jnp.bfloat16)
    low = lax.broadcasted_iota(jnp.int32, (nq, lanes), 1) < HEAD_DIM
    contract = (((1,), (1,)), ((), ()))
    for block in range(GRID_W // WIN_COLS):
        q = q_ref[0, :, WIN_COLS * block : WIN_COLS * (block + 1), :].reshape(nq, lanes)

        def keys(ref):
            if block == 0:
                got = jnp.concatenate([ref[0, :, GRID_W - WIN_COLS :, :], ref[0, :, :WIN_COLS, :]], 1)
            else:
                got = ref[0, :, WIN_COLS * (block - 1) : WIN_COLS * (block + 1), :]
            return got.reshape(nk, lanes)

        k = keys(k_ref)
        v = jnp.concatenate([keys(v_ref), ones], axis=1)
        halves = []
        for h in range(2):
            mine = low if h == 0 else jnp.logical_not(low)
            one = jnp.where(mine, q, jnp.zeros_like(q))
            near = lax.dot_general(one, k, contract, preferred_element_type=jnp.float32)
            near = near * factor + table[h, min(block, 1)]
            far = lax.dot_general(one, ck, contract, preferred_element_type=jnp.float32)
            far = far * factor + far_ref[2 * pair + h] * LOG2E
            top = jnp.maximum(
                jnp.max(near, axis=-1, keepdims=True), jnp.max(far, axis=-1, keepdims=True)
            )
            near = jnp.exp2(near - top).astype(jnp.bfloat16)
            far = jnp.exp2(far - top).astype(jnp.bfloat16)
            got = jnp.dot(near, v, preferred_element_type=jnp.float32) + jnp.dot(
                far, cv, preferred_element_type=jnp.float32
            )
            halves.append(got[:, :lanes] / got[:, lanes:])
        got = jnp.where(low, halves[0], halves[1]).astype(jnp.bfloat16)
        out_ref[0, :, WIN_COLS * block : WIN_COLS * (block + 1), :] = got.reshape(
            rows_dev, WIN_COLS, lanes
        )


def attention(query, pair, ctx_pair, rel_bias, ctx_bias):
    samples, rows_dev, _, cols = query.shape
    padded, ctx_count = pair.shape[1], ctx_pair.shape[1]
    heads = cols // HEAD_DIM
    lanes = 2 * HEAD_DIM
    pairs = cols // lanes
    nq, nk = rows_dev * WIN_COLS, padded * 2 * WIN_COLS
    flat = jnp.pad(rel_bias, ((0, 0), (0, 1), (0, 1))).reshape(heads, -1)
    flat = jnp.pad(flat, ((0, 0), (0, nk - flat.shape[1]))).reshape(pairs, 2, nk)
    token = lambda at: pl.BlockSpec((1, padded, GRID_W, lanes), lambda p, s: (s, 0, 0, p + at))
    far = lambda at: pl.BlockSpec((1, ctx_count, lanes), lambda p, s: (s, 0, p + at))
    own = pl.BlockSpec((1, rows_dev, GRID_W, lanes), lambda p, s: (s, 0, 0, p))
    scores = samples * heads * 4 * nq * (nk + ctx_count)
    return pl.pallas_call(
        attention_kernel,
        grid=(pairs, samples),
        out_shape=jax.ShapeDtypeStruct(query.shape, jnp.bfloat16),
        in_specs=[
            pl.BlockSpec((1, 2, nk), lambda p, s: (p, 0, 0)),
            pl.BlockSpec(memory_space=pltpu.SMEM),
            own,
            token(0),
            token(pairs),
            far(0),
            far(pairs),
        ],
        out_specs=own,
        scratch_shapes=[pltpu.VMEM((2, 2, nq, nk), jnp.float32)],
        cost_estimate=pl.CostEstimate(
            flops=scores * 512, bytes_accessed=8 * query.size * 2, transcendentals=scores
        ),
    )(flat, ctx_bias, query, pair, pair, ctx_pair, ctx_pair)


def on_device(
    latent,
    context,
    cond,
    ctx_cond,
    w_shift,
    w_scale,
    w_gate,
    norm_gain,
    w_query,
    w_key,
    w_value,
    w_out,
    rel_bias,
    ctx_bias,
):
    samples = latent.shape[0]
    rows_sp = w_shift.shape[0]
    local_cols = w_shift.shape[1]
    sp_index = lax.axis_index("sp")
    ada = silu_rows(jnp.concatenate([cond, ctx_cond[None, :]], axis=0))
    ada_rows = lax.dynamic_slice_in_dim(ada, sp_index * rows_sp, rows_sp, 1)
    partial_value = jnp.stack(
        [
            jnp.dot(ada_rows, weight, preferred_element_type=jnp.float32)
            for weight in (w_shift, w_scale, w_gate)
        ]
    )
    summed = lax.psum(partial_value, "sp")
    modulation = lax.all_gather(summed, "tp", axis=2, tiled=True)
    hidden = modulate_rows(
        latent, norm_gain, modulation[0, :samples, None, :], modulation[1, :samples, None, :]
    )
    w_triple = jnp.concatenate([w_query, w_key, w_value], axis=1)
    triple = jnp.dot(
        lax.all_gather(hidden, "tp", axis=1, tiled=True),
        w_triple,
        preferred_element_type=jnp.float32,
    ).astype(jnp.bfloat16)
    ctx_hidden = modulate_rows(context, norm_gain, modulation[0, samples], modulation[1, samples])
    w_pair = jnp.concatenate([w_key, w_value], axis=1)
    own_pair = jnp.dot(ctx_hidden, w_pair, preferred_element_type=jnp.float32).astype(jnp.bfloat16)
    ctx_pair = lax.all_gather(own_pair, "sp", axis=1, tiled=True)
    heads = local_cols // HEAD_DIM
    tokens_sp = triple.shape[1]
    rows_dev = tokens_sp // GRID_W
    rows_all = rows_dev * lax.axis_size("sp")
    reach = WIN_ROWS // 2
    query = triple[..., :local_cols].reshape(samples, rows_dev, GRID_W, local_cols)
    pair = triple[..., local_cols:].reshape(samples, rows_dev, GRID_W, 2 * local_cols)
    padded_pair = extended(pair, (("sp", 1),), reach)
    half = WIN_COLS // 2
    rolled = jnp.roll(query, half, axis=2)
    mixed = attention(rolled, padded_pair, ctx_pair, rel_bias, ctx_bias)
    attended = jnp.roll(mixed, -half, axis=2).reshape(samples, tokens_sp, local_cols)
    attended = attended.transpose(1, 0, 2)
    update = lax.psum_scatter(
        jnp.einsum("tsc,cd->tsd", attended, w_out, preferred_element_type=jnp.float32).astype(
            jnp.bfloat16
        ),
        "tp",
        scatter_dimension=0,
        tiled=True,
    ).astype(jnp.float32)
    gate = modulation[2, :samples, None, :]
    result = latent.astype(jnp.float32) + gate * update.transpose(1, 0, 2)
    return result.astype(jnp.bfloat16)


def solution(mesh):
    return jax.shard_map(
        on_device,
        mesh=mesh,
        in_specs=(
            P(None, ("sp", "tp"), None),
            P(None, "sp", None),
            P(),
            P(),
            P("sp", "tp"),
            P("sp", "tp"),
            P("sp", "tp"),
            P(),
            P(None, "tp"),
            P(None, "tp"),
            P(None, "tp"),
            P("tp", None),
            P("tp", None, None),
            P("tp"),
        ),
        out_specs=P(None, ("sp", "tp"), None),
        check_vma=False,
    )
```

time: 422 us -> 247 us (0.59); the launches traced: 414 us -> 246 us
  local copies, waits for them, and re-layouts: 149 us -> 7.8 us
  matrix products: 102 us -> 22.3 us
  waiting for transfers between devices: 77.3 us -> 123 us
  Pallas kernels: 0 us -> 16.4 us
  other arithmetic: 21.4 us -> 12.2 us
    dot_general x24 -> x0, matrix products: 80 us -> none  [the longest x4 20 us: on_device(): jnp.einsum('shnk,skhd->snhd', near_weight, block_pair[:, :, 1], preferred...]
    reshape x12 -> x1, local copies, waits for them, and re-layouts: 32.2 us -> 0.7 us  [attention(): jnp.pad(flat, ((0, 0), (0, nk - flat.shape[1]))).reshape(pairs, 2, nk)]
    add x4 -> x0, local copies, waits for them, and re-layouts: 30.2 us -> none  [on_device(): jnp.einsum('snhd,skhd->shnk', block_query, block_pair[:, :, 0], preferred...]
    unnamed x96 -> x15, local copies, waits for them, and re-layouts: 29.8 us -> 1.76 us
    ppermute x1, waiting for transfers between devices: 0.01 us -> 27.6 us  [extended(): after = lax.ppermute(first, axis, down)]
    all_gather x1, waiting for transfers between devices: 5.15 us -> 26.5 us  [on_device(): lax.all_gather(hidden, 'tp', axis=1, tiled=True)]
    slice x6, local copies, waits for them, and re-layouts: 22.4 us -> 1.32 us  [the longest x4 1.25 us: on_device(): jnp.roll(mixed, -half, axis=2).reshape(samples, tokens_sp, local_cols)]
    transpose x4 -> x0, local copies, waits for them, and re-layouts: 17 us -> none  [on_device(): jnp.einsum('rpa,hac,qkc->hrqpk', row_onehot, rel_bias, col_onehot, precis...]
  transfers between devices with their start and end apart: 5 -> 5, of which waited for: 3 -> 4; matrix products, arithmetic and copies ran while one was open for 22% -> 10% of each run, Pallas kernels for 0% -> 0%
where the time goes in v1:
time: 247 us; the launch traced here: 246 us
  waiting for transfers between devices  123 us (50%)
  blocking collectives  44.2 us (18%)
  matrix products  22.3 us (9%)
  Pallas kernels  16.4 us (7%)
  between operations  13.2 us (5%)
  other arithmetic  12.2 us (5%)
  local copies, waits for them, and re-layouts  7.8 us (3%)
  starting transfers between devices  6.88 us (3%)
    reduce_scatter x1, waiting for transfers between devices, on_device(): lax.psum_scatter(jnp.einsum('tsc,cd->tsd', attended, w_out, preferred_ele...  44.6 us
    psum x1, blocking collectives, on_device(): summed = lax.psum(partial_value, 'sp')  38.9 us
    ppermute x1, waiting for transfers between devices, extended(): after = lax.ppermute(first, axis, down)  27.6 us
    all_gather x1, waiting for transfers between devices, on_device(): lax.all_gather(hidden, 'tp', axis=1, tiled=True)  26.5 us
    ppermute x1, waiting for transfers between devices, extended(): before = lax.ppermute(last, axis, up)  24.4 us
    pallas_call x1, Pallas kernels, attention(): pl.pallas_call(attention_kernel, grid=(pairs, samples), out_shape=jax.Sha...  16.4 us
    dot_general x1, matrix products, on_device(): jnp.dot(lax.all_gather(hidden, 'tp', axis=1, tiled=True), w_triple, prefe...  10.7 us
    ppermute x1, starting transfers between devices, extended(): before = lax.ppermute(last, axis, up)  5.52 us
  transfers between devices with their start and end apart: 5, of which 4 were waited for; matrix products, arithmetic and copies ran while one was open for 10% of the time, Pallas kernels for 0%

profile of v1, /device:TPU:0, one launch (start us, length us, event | category | flops | bytes accessed | tf_op | source)
XLA Modules:
  0.0 246.1 jit_solution(4152016299215800951)
XLA Ops:
  6.6 0.8 broadcast_in_dim.2
  7.4 0.8 maximum_convert_fusion
  8.2 1.1 convolution_bitcast_fusion
  9.3 1.1 convolution_bitcast_fusion.1
  10.4 1.1 convolution_bitcast_fusion.2
  11.5 38.9 %psum.7 = f32[3,3,512]{2,1,0:T(4,128)S(1)} all-reduce(f32[3,3,512]{2,1,0:T(4,128)S(1)} %pad_maximum_fusion.3), channel_id=1, replica_groups=mesh['sp'=8,'tp'=4] {'sp'}, use_global_device_ids=true, to_apply=%region_0.1 | all-reduce | flops 4608 | bytes 36864 | tf_op jit(solution)/shard_map/psum | solution.py:178
  50.3 5.3 %all_gather.9 = f32[3,3,2048]{2,1,0:T(4,128)S(1)} all-gather(f32[3,3,512]{2,1,0:T(4,128)S(1)} %psum.7), channel_id=1, replica_groups=mesh['sp'=8,'tp'=4] {'tp'}, dimensions={2}, use_global_device_ids=true | all-gather | bytes 92160 | tf_op jit(solution)/shard_map/all_gather | solution.py:179
  55.7 1.5 fusion.7
  57.2 1.5 fusion.11
  58.8 1.2 fusion.15
  60.0 4.0 %fusion.14 = bf16[2,64,1024]{2,1,0:T(8,128)(2,1)} fusion(bf16[2048,512]{1,0:T(8,128)(2,1)} %param.24, bf16[2048,512]{1,0:T(8,128)(2,1)} %param.23, bf16[2,64,2048]{2,1,0:T(8,128)(2,1)} %param.15, f32[2048]{0:T(1024)S(1)} %bitcast.45, f32[2048]{0:T(1024)S(1)} %bitcast.44, f32[2048]{0:T(1024)S(1)} %copy-done.6, f32[2,64]{1,0:T(2,128)S(1)} %add_rsqrt_fusion), kind=kOutput, calls=%fused_computation.23 | convolution fusion | flops 546963456 | bytes 5005824 | tf_op jit(solution)/shard_map/dot_general | solution.py:191
  64.1 26.5 %all-gather.3.cloned.1.call-done = bf16[2,512,2048]{2,1,0:T(8,128)(2,1)} async-done(((bf16[2,128,2048]{2,1,0:T(8,128)(2,1)}), bf16[2,512,2048]{2,1,0:T(8,128)(2,1)}) %all-gather.3.cloned.1.call-update) | async-done | bytes 4194320 | tf_op jit(solution)/shard_map/all_gather | solution.py:185
  90.6 10.7 %fusion.6 = bf16[2,512,1536]{2,1,0:T(8,128)(2,1)S(1)} fusion(bf16[2,512,2048]{2,1,0:T(8,128)(2,1)} %all-gather.3.cloned.1.call-done, bf16[2048,512]{1,0:T(8,128)(2,1)} %param.24, bf16[2048,512]{1,0:T(8,128)(2,1)} %param.23, bf16[2048,512]{1,0:T(8,128)(2,1)} %param.22), kind=kOutput, calls=%fused_computation.9 | convolution fusion | flops 6462898176 | bytes 13631488 | tf_op jit(solution)/shard_map/dot_general | solution.py:184
  101.3 0.2 slice.62
  101.6 1.4 copy-done.4
  103.0 1.6 fusion.32
  104.6 0.4 copy-done.1
  105.0 1.3 collective-permute-start.1
  106.2 5.5 %collective-permute-start = (bf16[2,4,64,1024]{3,2,1,0:T(8,128)(2,1)}, bf16[2,4,64,1024]{3,2,1,0:T(8,128)(2,1)}, u32[]{:S(2)}, u32[]{:S(2)}) collective-permute-start(bf16[2,4,64,1024]{3,2,1,0:T(8,128)(2,1)} %get-tuple-element.5), channel_id=1, source_target_pairs={{0,4},{4,8},{8,12},{12,16},{16,20},{20,24},{24,28},{1,5},{5,9},{9,... | collective-permute-start | bytes 3145736 | tf_op jit(solution)/shard_map/ppermute | solution.py:24
  111.8 0.7 reshape.42.bias_ref
  112.5 1.3 slice.59
  113.9 1.1 pad_maximum_fusion.1.q_ref
  115.0 27.6 %collective-permute-done.1 = bf16[2,4,64,1024]{3,2,1,0:T(8,128)(2,1)} collective-permute-done((bf16[2,4,64,1024]{3,2,1,0:T(8,128)(2,1)}, bf16[2,4,64,1024]{3,2,1,0:T(8,128)(2,1)}, u32[]{:S(2)}, u32[]{:S(2)}) %collective-permute-start.1) | collective-permute-done | bytes 1048608 | tf_op jit(solution)/shard_map/ppermute | solution.py:25
  142.5 24.4 %collective-permute-done = bf16[2,4,64,1024]{3,2,1,0:T(8,128)(2,1)} collective-permute-done((bf16[2,4,64,1024]{3,2,1,0:T(8,128)(2,1)}, bf16[2,4,64,1024]{3,2,1,0:T(8,128)(2,1)}, u32[]{:S(2)}, u32[]{:S(2)}) %collective-permute-start) | collective-permute-done | bytes 1048608 | tf_op jit(solution)/shard_map/ppermute | solution.py:24
  166.9 3.4 %pad_maximum_fusion.k_ref.v_ref = bf16[2,16,64,1024]{3,2,1,0:T(8,128)(2,1)} fusion(bf16[2,4,64,1024]{3,2,1,0:T(8,128)(2,1)} %collective-permute-done.1, bf16[2,8,64,1024]{3,2,1,0:T(8,128)(2,1)S(1)} %bitcast.40, bf16[2,4,64,1024]{3,2,1,0:T(8,128)(2,1)} %collective-permute-done), kind=kLoop, calls=%fused_computation.6 | loop fusion | flops 4194304 | bytes 8388608 | tf_op jit(solution)/shard_map/concatenate | solution.py:26
  170.3 16.4 %shard_map.136 = bf16[2,8,64,512]{3,2,1,0:T(8,128)(2,1)} custom-call(f32[4,2,512]{2,1,0:T(2,128)} %reshape.42.bias_ref, f32[8]{0:T(128)} %far_ref.1, bf16[2,8,64,512]{3,2,1,0:T(8,128)(2,1)} %pad_maximum_fusion.1.q_ref, bf16[2,16,64,1024]{3,2,1,0:T(8,128)(2,1)} %pad_maximum_fusion.k_ref.v_ref, bf16[2,16,64,1024]{3,2,1,0:T(8,128)(2,1)} %pad_maximum_fusion.k_ref.v_ref, ...), custom_call_target="tpu_custom_call" | custom-call | flops 4294967296 | bytes 8388608 | tf_op jit(solution)/shard_map/pallas_call | solution.py:129
  186.7 0.9 slice-done
  187.6 0.4 slice-done.1
  187.9 0.1 pad_maximum_fusion.2
  188.1 4.3 %convolution_convert_fusion = bf16[512,2,2048]{2,0,1:T(8,128)(2,1)} fusion(bf16[512,2,512]{2,0,1:T(8,128)(2,1)S(1)} %bitcast.43, bf16[512,2048]{1,0:T(8,128)(2,1)S(1)} %copy-done), kind=kOutput, calls=%fused_computation.10 | convolution fusion | flops 2149580800 | bytes 7340032 | tf_op jit(solution)/shard_map/tsc,cd->tsd/dot_general | solution.py:207
  192.4 44.6 %reduce-scatter.2.cloned.1.call-done = bf16[128,2,2048]{2,0,1:T(8,128)(2,1)} async-done(((bf16[512,2,2048]{2,0,1:T(8,128)(2,1)}), bf16[128,2,2048]{2,0,1:T(8,128)(2,1)}) %reduce-scatter.2.cloned.1.call-update) | async-done | bytes 1048592 | tf_op jit(solution)/shard_map/reduce_scatter | solution.py:206
  237.0 2.6 %fusion.12 = bf16[2,128,2048]{2,1,0:T(8,128)(2,1)} fusion(bf16[2,128,2048]{2,1,0:T(8,128)(2,1)S(1)} %copy-done.3, bf16[128,2,2048]{2,0,1:T(8,128)(2,1)} %reduce-scatter.2.cloned.1.call-done, f32[2,2048]{1,0:T(2,128)S(1)} %get-tuple-element.7), kind=kLoop, calls=%fused_computation.19 | loop fusion | flops 2621440 | bytes 3162112 | tf_op jit(solution)/shard_map/convert_element_type | solution.py:216
  (30 shorter events, 0.3 us)
Async XLA Ops:
  6.5 181.5 %copy-start = (bf16[512,2048]{1,0:T(8,128)(2,1)S(1)}, bf16[512,2048]{1,0:T(8,128)(2,1)}, u32[]{:S(2)}) copy-start(bf16[512,2048]{1,0:T(8,128)(2,1)} %param.25) | copy-start | bytes 6291460
  6.5 50.6 %copy-start.3 = (bf16[2,128,2048]{2,1,0:T(8,128)(2,1)S(1)}, bf16[2,128,2048]{2,1,0:T(8,128)(2,1)}, u32[]{:S(2)}) copy-start(bf16[2,128,2048]{2,1,0:T(8,128)(2,1)} %param.14) | copy-start | bytes 3145732
  6.5 50.7 %copy-start.6 = (f32[2048]{0:T(1024)S(1)}, f32[2048]{0:T(1024)}, u32[]{:S(2)}) copy-start(f32[2048]{0:T(1024)} %param.21) | copy-start | bytes 24580
  6.5 84.1 %all-gather.3.cloned.1.call-start = ((), (), s32[]{:S(2)}) async-start(), calls=%async_computation.1 | async-start | bytes 5242880 | tf_op jit(solution)/shard_map/all_gather | solution.py:185
  58.7 111.6 %all-gather.5.cloned.1.call-start = ((), (), s32[]{:S(2)}) async-start(), calls=%async_computation.2 | async-start | bytes 2359296 | tf_op jit(solution)/shard_map/all_gather | solution.py:192
  64.1 172.9 %reduce-scatter.2.cloned.1.call-start = ((), (), s32[]{:S(2)}) async-start(), calls=%async_computation.3 | async-start | bytes 5242880 | tf_op jit(solution)/shard_map/reduce_scatter | solution.py:206
  101.3 1.6 copy-start.4
  103.0 2.0 copy-start.1
  103.0 8.8 %copy-start.5 = (f32[8,15,31]{2,0,1:T(8,128)S(1)}, f32[8,15,31]{2,0,1:T(8,128)}, u32[]{:S(2)}) copy-start(f32[8,15,31]{2,0,1:T(8,128)} %param.26) | copy-start | bytes 44644
  105.0 37.6 %collective-permute-start.1 = (bf16[2,4,64,1024]{3,2,1,0:T(8,128)(2,1)}, bf16[2,4,64,1024]{3,2,1,0:T(8,128)(2,1)}, u32[]{:S(2)}, u32[]{:S(2)}) collective-permute-start(bf16[2,4,64,1024]{3,2,1,0:T(8,128)(2,1)} %get-tuple-element.6), channel_id=1, source_target_pairs={{4,0},{8,4},{12,8},{16,12},{20,16},{24,20},{28,24},{5,1},{9,5},{13... | collective-permute-start | bytes 3145736 | tf_op jit(solution)/shard_map/ppermute | solution.py:25
  106.2 60.7 %collective-permute-start = (bf16[2,4,64,1024]{3,2,1,0:T(8,128)(2,1)}, bf16[2,4,64,1024]{3,2,1,0:T(8,128)(2,1)}, u32[]{:S(2)}, u32[]{:S(2)}) collective-permute-start(bf16[2,4,64,1024]{3,2,1,0:T(8,128)(2,1)} %get-tuple-element.5), channel_id=1, source_target_pairs={{0,4},{4,8},{8,12},{12,16},{16,20},{20,24},{24,28},{1,5},{5,9},{9,... | collective-permute-start | bytes 3145736 | tf_op jit(solution)/shard_map/ppermute | solution.py:24
  113.8 53.1 %copy-start.2 = (bf16[2,512,1024]{2,1,0:T(8,128)(2,1)S(1)}, bf16[2,512,1024]{2,1,0:T(8,128)(2,1)}, u32[]{:S(2)}) copy-start(bf16[2,512,1024]{2,1,0:T(8,128)(2,1)} %copy-done.1) | copy-start | bytes 6291460
  186.7 0.9 slice-start
  186.7 1.3 slice-start.1
Sparse Core Ops, SparseCore 0:
  58.8 31.7 all-gather.2
  92.8 75.8 all-gather.4
  192.5 44.4 reduce-scatter.1

commit v2 on v1

--- a/solution.py
+++ b/solution.py
@@ -216,9 +216,335 @@
     return result.astype(jnp.bfloat16)
 
 
+MESH = pl.DeviceIdType.MESH
+
+
+def entry_barrier(peers):
+    barrier = pltpu.get_barrier_semaphore()
+    for device, there in peers:
+        @pl.when(there)
+        def _():
+            pl.semaphore_signal(barrier, inc=1, device_id=device, device_id_type=MESH)
+    pl.semaphore_wait(barrier, sum(jnp.where(there, 1, 0) for _, there in peers))
+
+
+def modulation_kernel(ada_ref, a_ref, b_ref, c_ref, out_ref, part, got, total, full, s1, r1, s2, r2):
+    sp, tp = lax.axis_index("sp"), lax.axis_index("tp")
+    n_sp, n_tp = lax.axis_size("sp"), lax.axis_size("tp")
+    over_sp = [lax.rem(sp + k, n_sp) for k in range(1, n_sp)]
+    over_tp = [lax.rem(tp + k, n_tp) for k in range(1, n_tp)]
+    entry_barrier([((p, tp), sp >= 0) for p in over_sp] + [((sp, p), sp >= 0) for p in over_tp])
+    for at, weight in enumerate((a_ref, b_ref, c_ref)):
+        value = jnp.dot(ada_ref[...], weight[...], preferred_element_type=jnp.float32)
+        part[8 * at : 8 * at + 8, :] = value[:8]
+
+    def first(k, peer):
+        return pltpu.make_async_remote_copy(
+            src_ref=part, dst_ref=got.at[k], send_sem=s1.at[k], recv_sem=r1.at[k],
+            device_id=(peer, tp), device_id_type=MESH,
+        )
+
+    def second(k, peer):
+        return pltpu.make_async_remote_copy(
+            src_ref=total, dst_ref=full.at[k], send_sem=s2.at[k], recv_sem=r2.at[k],
+            device_id=(sp, peer), device_id_type=MESH,
+        )
+
+    copies = [first(k, peer) for k, peer in enumerate(over_sp)]
+    for copy in copies:
+        copy.start()
+    value = part[...]
+    for k, copy in enumerate(copies):
+        copy.wait()
+        value = value + got[k]
+    total[...] = value
+    copies = [second(k, peer) for k, peer in enumerate(over_tp)]
+    for copy in copies:
+        copy.start()
+    out_ref[0] = value
+    for k, copy in enumerate(copies):
+        copy.wait()
+        out_ref[k + 1] = full[k]
+
+
+def modulation_vectors(ada_rows, weights):
+    n_sp, n_tp = lax.axis_size("sp"), lax.axis_size("tp")
+    cols = weights[0].shape[1]
+    block = (24, cols)
+    ada_rows = jnp.pad(ada_rows, ((0, 16 - ada_rows.shape[0]), (0, 0)))
+    got = pl.pallas_call(
+        modulation_kernel,
+        out_shape=jax.ShapeDtypeStruct((n_tp,) + block, jnp.float32),
+        in_specs=[pl.BlockSpec(memory_space=pltpu.VMEM)] * 4,
+        out_specs=pl.BlockSpec(memory_space=pltpu.VMEM),
+        scratch_shapes=[
+            pltpu.VMEM(block, jnp.float32),
+            pltpu.VMEM((n_sp - 1,) + block, jnp.float32),
+            pltpu.VMEM(block, jnp.float32),
+            pltpu.VMEM((n_tp - 1,) + block, jnp.float32),
+            pltpu.SemaphoreType.DMA((n_sp - 1,)),
+            pltpu.SemaphoreType.DMA((n_sp - 1,)),
+            pltpu.SemaphoreType.DMA((n_tp - 1,)),
+            pltpu.SemaphoreType.DMA((n_tp - 1,)),
+        ],
+        compiler_params=pltpu.CompilerParams(collective_id=1, has_side_effects=True),
+    )(ada_rows, *weights)
+    tp = lax.axis_index("tp")
+    order = lax.rem(tp + n_tp - jnp.arange(n_tp), n_tp)
+    got = jnp.take(got, order, axis=0)
+    return got.transpose(1, 0, 2).reshape(3, 8, n_tp * cols)
+
+
+def gather_kernel(latent_ref, ctx_ref, ext_ref, all_ref, own_sem, s_ext, r_ext, s_ctx, r_ctx):
+    sp, tp = lax.axis_index("sp"), lax.axis_index("tp")
+    n_sp = lax.axis_size("sp")
+    y, c = tp // 2, lax.rem(tp, 2)
+    sib, across = y * 2 + 1 - c, (1 - y) * 2 + c
+    always = sp >= 0
+    has_up, has_down = sp > 0, sp < n_sp - 1
+    direct = y * c + (1 - y) * (6 + c)
+    indirect = (1 - y) * c + y * (6 + c)
+    has_direct = ((y == 1) & has_up) | ((y == 0) & has_down)
+    has_indirect = ((y == 0) & has_up) | ((y == 1) & has_down)
+    toward = sp + 2 * y - 1
+    away = sp - 2 * y + 1
+    here, there = (sp, sib), (sp, across)
+    own_slot, across_slot = 2 + tp, 2 + across
+    x_peer = sp + 1 - 2 * lax.rem(sp, 2)
+    entry_barrier(
+        [
+            (here, always),
+            (there, always),
+            ((x_peer, tp), always),
+            ((sp + 2, tp), sp + 2 < n_sp),
+            ((sp - 2, tp), sp >= 2),
+            ((sp + 1, tp), has_down & (lax.rem(sp, 2) == 1)),
+            ((sp - 1, tp), has_up & (lax.rem(sp, 2) == 0)),
+        ]
+    )
+
+    def piece(flow, s, device, slot, own=False, at=None):
+        return pltpu.make_async_remote_copy(
+            src_ref=latent_ref.at[s] if own else ext_ref.at[s, slot if at is None else at],
+            dst_ref=ext_ref.at[s, slot],
+            send_sem=s_ext.at[flow, s],
+            recv_sem=r_ext.at[flow, s],
+            device_id=device,
+            device_id_type=MESH,
+        )
+
+    sends = []
+
+    def send(cond, copy):
+        sends.append((cond, copy))
+
+        @pl.when(cond)
+        def _():
+            copy.start()
+
+    def arrived(cond, copy):
+        @pl.when(cond)
+        def _():
+            copy.wait_recv()
+
+    blocks = {}
+
+    def block(at, way, device, own=False):
+        return pltpu.make_async_remote_copy(
+            src_ref=ctx_ref if own else all_ref.at[at],
+            dst_ref=all_ref.at[at],
+            send_sem=s_ctx.at[at, way],
+            recv_sem=r_ctx.at[at],
+            device_id=device,
+            device_id_type=MESH,
+        )
+
+    up, down = (sp + 2, tp), (sp - 2, tp)
+    can_up, can_down = sp + 2 < n_sp, sp >= 2
+    mine = [pltpu.make_async_copy(latent_ref.at[s], ext_ref.at[s, own_slot], own_sem.at[s]) for s in range(2)]
+    mine.append(pltpu.make_async_copy(ctx_ref, all_ref.at[sp], own_sem.at[2]))
+    send(always, block(sp, 0, (x_peer, tp), True))
+    send(can_up, block(sp, 1, up, True))
+    send(can_down, block(sp, 2, down, True))
+    for s in range(2):
+        send(always, piece(1, s, there, own_slot, True))
+        send(has_indirect, piece(2, s, (toward, tp), direct, True))
+    for s in range(2):
+        send(always, piece(0, s, here, own_slot, True))
+    for copy in mine:
+        copy.start()
+    arrived(always, block(x_peer, 0, (x_peer, tp)))
+    send(can_up, block(x_peer, 1, up))
+    send(can_down, block(x_peer, 2, down))
+
+    def relay(hop):
+        for e in range(2):
+            at = sp - lax.rem(sp, 2) - 2 * hop + e
+            arrived(at >= 0, block(lax.max(at, 0), 1, up))
+            send((at >= 0) & can_up, block(lax.max(at, 0), 1, up))
+            low = sp - lax.rem(sp, 2) + 2 * hop + e
+            arrived(low < n_sp, block(lax.min(low, n_sp - 1), 2, down))
+            send((low < n_sp) & can_down, block(lax.min(low, n_sp - 1), 2, down))
+
+    arrived(always, piece(1, 0, there, across_slot))
+    send(always, piece(3, 0, here, across_slot))
+    arrived(has_direct, piece(2, 0, here, direct))
+    send(has_direct, piece(5, 0, there, direct))
+    send(has_direct, piece(6, 0, here, direct))
+    relay(1)
+    arrived(always, piece(1, 1, there, across_slot))
+    send(has_direct, piece(4, 1, (away, tp), indirect, at=across_slot))
+    send(always, piece(3, 1, here, across_slot))
+    arrived(has_direct, piece(2, 1, here, direct))
+    send(has_direct, piece(6, 1, here, direct))
+    for hop in range(2, n_sp // 2):
+        relay(hop)
+    arrived(has_indirect, piece(5, 0, there, indirect))
+    send(has_indirect, piece(7, 0, here, indirect))
+    arrived(has_indirect, piece(4, 1, there, indirect))
+    send(has_indirect, piece(7, 1, here, indirect))
+    for s in range(2):
+        arrived(always, piece(0, s, here, own_slot))
+        arrived(always, piece(3, s, here, own_slot))
+        arrived(has_direct, piece(6, s, here, direct))
+        arrived(has_indirect, piece(7, s, here, indirect))
+    for cond, copy in sends:
+        @pl.when(cond)
+        def _():
+            copy.wait_send()
+    for copy in mine:
+        copy.wait()
+
+
+def gather_tokens(latent, ctx_pair):
+    n_sp = lax.axis_size("sp")
+    samples, tokens, width = latent.shape
+    return pl.pallas_call(
+        gather_kernel,
+        out_shape=(
+            jax.ShapeDtypeStruct((samples, 8, tokens, width), latent.dtype),
+            jax.ShapeDtypeStruct((n_sp,) + ctx_pair.shape, ctx_pair.dtype),
+        ),
+        in_specs=[pl.BlockSpec(memory_space=pl.ANY)] * 2,
+        out_specs=[pl.BlockSpec(memory_space=pl.ANY)] * 2,
+        scratch_shapes=[
+            pltpu.SemaphoreType.DMA((3,)),
+            pltpu.SemaphoreType.DMA((8, 2)),
+            pltpu.SemaphoreType.DMA((8, 2)),
+            pltpu.SemaphoreType.DMA((n_sp, 3)),
+            pltpu.SemaphoreType.DMA((n_sp,)),
+        ],
+        compiler_params=pltpu.CompilerParams(collective_id=2, has_side_effects=True),
+    )(latent, ctx_pair)
+
+
+def scatter_kernel(parts_ref, out_ref, got, summed, far, s1, r1, s2, r2):
+    sp, tp = lax.axis_index("sp"), lax.axis_index("tp")
+    y, c = tp // 2, lax.rem(tp, 2)
+    sib, across = y * 2 + 1 - c, (1 - y) * 2 + c
+    sib_across = (1 - y) * 2 + 1 - c
+    entry_barrier([((sp, sib), sp >= 0), ((sp, across), sp >= 0)])
+    chunks = far.shape[0]
+    rows = far.shape[1]
+
+    def near(k):
+        at = k % chunks
+        target = sib_across if k < chunks else sib
+        return pltpu.make_async_remote_copy(
+            src_ref=parts_ref.at[target, pl.ds(at * rows, rows)],
+            dst_ref=got.at[k],
+            send_sem=s1.at[k], recv_sem=r1.at[k],
+            device_id=(sp, sib), device_id_type=MESH,
+        )
+
+    def cross(k):
+        return pltpu.make_async_remote_copy(
+            src_ref=summed.at[k],
+            dst_ref=far.at[k],
+            send_sem=s2.at[k], recv_sem=r2.at[k],
+            device_id=(sp, across), device_id_type=MESH,
+        )
+
+    for k in range(2 * chunks):
+        near(k).start()
+    for k in range(chunks):
+        near(k).wait()
+        mine = parts_ref[across, k * rows : (k + 1) * rows, :].astype(jnp.float32)
+        summed[k] = (mine + got[k].astype(jnp.float32)).astype(jnp.bfloat16)
+        cross(k).start()
+    for k in range(chunks):
+        near(chunks + k).wait()
+        cross(k).wait()
+        mine = parts_ref[tp, k * rows : (k + 1) * rows, :].astype(jnp.float32)
+        mine = mine + got[chunks + k].astype(jnp.float32) + far[k].astype(jnp.float32)
+        out_ref[k * rows : (k + 1) * rows, :] = mine
+
+
+def scatter_sum(parts):
+    _, tokens, width = parts.shape
+    chunks = 4
+    rows = tokens // chunks
+    sems = [pltpu.SemaphoreType.DMA((2 * chunks,))] * 2 + [pltpu.SemaphoreType.DMA((chunks,))] * 2
+    return pl.pallas_call(
+        scatter_kernel,
+        out_shape=jax.ShapeDtypeStruct((tokens, width), jnp.float32),
+        in_specs=[pl.BlockSpec(memory_space=pltpu.VMEM)],
+        out_specs=pl.BlockSpec(memory_space=pltpu.VMEM),
+        scratch_shapes=[
+            pltpu.VMEM((2 * chunks, rows, width), jnp.bfloat16),
+            pltpu.VMEM((chunks, rows, width), jnp.bfloat16),
+            pltpu.VMEM((chunks, rows, width), jnp.bfloat16),
+        ]
+        + sems,
+        compiler_params=pltpu.CompilerParams(
+            collective_id=3, has_side_effects=True, vmem_limit_bytes=40 * 2**20
+        ),
+    )(parts)
+
+
+def on_four(
+    latent, context, cond, ctx_cond, w_shift, w_scale, w_gate, norm_gain,
+    w_query, w_key, w_value, w_out, rel_bias, ctx_bias,
+):
+    samples, tokens, width = latent.shape
+    n_sp, n_tp = lax.axis_size("sp"), lax.axis_size("tp")
+    rows_sp, local_cols = w_shift.shape
+    sp = lax.axis_index("sp")
+    ada = silu_rows(jnp.concatenate([cond, ctx_cond[None, :]], axis=0))
+    ada_rows = lax.dynamic_slice_in_dim(ada, sp * rows_sp, rows_sp, 1)
+    modulation = modulation_vectors(ada_rows, (w_shift, w_scale, w_gate))
+    ctx_hidden = modulate_rows(context, norm_gain, modulation[0, samples], modulation[1, samples])
+    w_pair = jnp.concatenate([w_key, w_value], axis=1)
+    own_pair = jnp.dot(ctx_hidden, w_pair, preferred_element_type=jnp.float32).astype(jnp.bfloat16)
+    ext, ctx_all = gather_tokens(latent, own_pair)
+    ctx_pair = ctx_all.transpose(1, 0, 2, 3).reshape(samples, -1, 2 * local_cols)
+    hidden = modulate_rows(
+        ext, norm_gain, modulation[0, :samples, None, None, :], modulation[1, :samples, None, None, :]
+    )
+    slot = jnp.arange(8)[None, :, None, None]
+    valid = ((slot >= 2) | (sp > 0)) & ((slot < 6) | (sp < n_sp - 1))
+    hidden = jnp.where(valid, hidden, jnp.zeros_like(hidden))
+    rows_dev = n_tp * tokens // GRID_W
+    pair = jnp.dot(hidden, w_pair, preferred_element_type=jnp.float32).astype(jnp.bfloat16)
+    pair = pair.reshape(samples, 2 * rows_dev, GRID_W, 2 * local_cols)
+    query = jnp.dot(hidden[:, 2:6], w_query, preferred_element_type=jnp.float32)
+    query = query.astype(jnp.bfloat16).reshape(samples, rows_dev, GRID_W, local_cols)
+    half = WIN_COLS // 2
+    rolled = jnp.roll(query, half, axis=2)
+    mixed = attention(rolled, pair, ctx_pair, rel_bias, ctx_bias)
+    attended = jnp.roll(mixed, -half, axis=2).reshape(samples, n_tp, tokens, local_cols)
+    attended = attended.transpose(1, 0, 2, 3).reshape(n_tp, samples * tokens, local_cols)
+    parts = jnp.dot(attended, w_out, preferred_element_type=jnp.float32).astype(jnp.bfloat16)
+    update = scatter_sum(parts).reshape(samples, tokens, width)
+    gate = modulation[2, :samples, None, :]
+    return (latent.astype(jnp.float32) + gate * update).astype(jnp.bfloat16)
+
+
 def solution(mesh):
+    shape = dict(mesh.shape)
+    quick = shape["tp"] == 4 and shape["sp"] % 2 == 0
     return jax.shard_map(
-        on_device,
+        on_four if quick else on_device,
         mesh=mesh,
         in_specs=(
             P(None, ("sp", "tp"), None),

time: 247 us -> 169 us (0.68)
  waiting for transfers between devices: 123 us -> 0 us
  Pallas kernels: 16.4 us -> 126 us
  blocking collectives: 44.2 us -> 0 us
  between operations: 13.2 us -> 0.3 us
  starting transfers between devices: 6.88 us -> 0 us
  local copies, waits for them, and re-layouts: 7.8 us -> 12.8 us
  other arithmetic: 12.2 us -> 8.66 us
    pallas_call x0 -> x3, Pallas kernels: none -> 110 us  [the longest x1 63 us: gather_tokens(): pl.pallas_call(gather_kernel, out_shape=(jax.ShapeDtypeStruct((samples, 8...]
    ppermute x2 -> x0, waiting for transfers between devices: 52 us -> none  [the longest x1 27.6 us: extended(): after = lax.ppermute(first, axis, down)]
    reduce_scatter x1 -> x0, waiting for transfers between devices: 44.6 us -> none  [on_device(): lax.psum_scatter(jnp.einsum('tsc,cd->tsd', attended, w_out, preferred_ele...]
    psum x1 -> x0, blocking collectives: 38.9 us -> none  [on_device(): summed = lax.psum(partial_value, 'sp')]
    all_gather x2 -> x0, waiting for transfers between devices: 26.5 us -> none  [the longest x1 26.5 us: on_device(): lax.all_gather(hidden, 'tp', axis=1, tiled=True)]
    ppermute x2 -> x0, starting transfers between devices: 6.8 us -> none  [the longest x1 5.52 us: extended(): before = lax.ppermute(last, axis, up)]
    all_gather x1 -> x0, blocking collectives: 5.31 us -> none  [on_device(): modulation = lax.all_gather(summed, 'tp', axis=2, tiled=True)]
    concatenate x3 -> x2, other arithmetic: 4.56 us -> 1.19 us  [the longest x1 1.09 us: on_four(): rolled = jnp.roll(query, half, axis=2)]
  transfers between devices with their start and end apart: 5 -> 0, of which waited for: 4 -> 0; matrix products, arithmetic and copies ran while one was open for 10% -> 0% of each run, Pallas kernels for 0% -> 0%
where the time goes in v2:
time: 169 us; the launch traced here: 168 us
  Pallas kernels  126 us (75%)
  matrix products  20.5 us (12%)
  local copies, waits for them, and re-layouts  12.8 us (8%)
  other arithmetic  8.66 us (5%)
    pallas_call x1, Pallas kernels, gather_tokens(): pl.pallas_call(gather_kernel, out_shape=(jax.ShapeDtypeStruct((samples, 8...  63 us
    pallas_call x1, Pallas kernels, scatter_sum(): pl.pallas_call(scatter_kernel, out_shape=jax.ShapeDtypeStruct((tokens, wi...  28.1 us
    pallas_call x1, Pallas kernels, modulation_vectors(): pl.pallas_call(modulation_kernel, out_shape=jax.ShapeDtypeStruct((n_tp,)...  18.7 us
    pallas_call x1, Pallas kernels, attention(): pl.pallas_call(attention_kernel, grid=(pairs, samples), out_shape=jax.Sha...  16.3 us
    dot_general x1, matrix products, on_four(): jnp.dot(hidden, w_pair, preferred_element_type=jnp.float32)  14.3 us
    reduce_sum x2, other arithmetic, modulate_rows(): jnp.mean(floats * floats, axis=-1, keepdims=True) + EPSILON  5.27 us
    unnamed x22, local copies, waits for them, and re-layouts  4.72 us

profile of v2, /device:TPU:0, one launch (start us, length us, event | category | flops | bytes accessed | tf_op | source)
XLA Modules:
  0.0 168.4 jit_solution(17112690927900151512)
XLA Ops:
  0.0 0.8 broadcast_in_dim.31
  0.8 0.7 maximum_convert_fusion
  1.6 0.6 pad.8.ada_ref
  2.2 18.7 %shard_map.136 = f32[4,24,512]{2,1,0:T(8,128)} custom-call(bf16[16,256]{1,0:T(8,128)(2,1)} %pad.8.ada_ref, bf16[256,512]{1,0:T(8,128)(2,1)} %a_ref.1, bf16[256,512]{1,0:T(8,128)(2,1)} %b_ref.1, bf16[256,512]{1,0:T(8,128)(2,1)} %c_ref.1), custom_call_target="tpu_custom_call" | custom-call | tf_op jit(solution)/shard_map/pallas_call | solution.py:275
  20.9 1.5 gather_fusion
  22.4 0.1 select_bitcast_fusion
  22.5 0.1 copy.18
  22.7 0.1 reshape.109
  22.9 2.1 %constant_dynamic-update-slice_fusion.1 = bf16[2048,1024]{1,0:T(8,128)(2,1)S(1)} fusion(bf16[2048,512]{1,0:T(8,128)(2,1)} %param.23), kind=kLoop, calls=%fused_computation.45 | loop fusion | bytes 4194304
  24.9 0.1 copy-done.3
  25.0 0.3 constant_dynamic-update-slice_fusion
  25.4 0.2 fusion.22
  25.6 1.7 %copy-done.5 = bf16[2048,1024]{1,0:T(8,128)(2,1)} copy-done((bf16[2048,1024]{1,0:T(8,128)(2,1)}, bf16[2048,1024]{1,0:T(8,128)(2,1)S(1)}, u32[]{:S(2)}) %copy-start.5) | copy-done | bytes 4194328
  27.3 1.5 fusion.19.ctx_ref
  28.8 63.0 %shard_map.137 = (bf16[2,8,128,2048]{3,2,1,0:T(8,128)(2,1)}, bf16[8,2,64,1024]{3,2,1,0:T(8,128)(2,1)}) custom-call(bf16[2,128,2048]{2,1,0:T(8,128)(2,1)} %latent_ref.1, bf16[2,64,1024]{2,1,0:T(8,128)(2,1)} %fusion.19.ctx_ref), custom_call_target="tpu_custom_call" | custom-call | tf_op jit(solution)/shard_map/pallas_call | solution.py:422
  91.8 5.1 %fusion = f32[2,8,128]{2,1,0:T(8,128)S(1)} fusion(bf16[2,8,128,2048]{3,2,1,0:T(8,128)(2,1)} %get-tuple-element.7), kind=kLoop, calls=%fused_computation.3 | loop fusion | flops 12580864 | bytes 8396800 | tf_op jit(solution)/shard_map/reduce_sum | solution.py:36
  97.0 0.0 copy-start.8
  97.0 14.3 %fusion.10 = bf16[2,8,128,1024]{3,2,1,0:T(8,128)(2,1)} fusion(bf16[2048,1024]{1,0:T(8,128)(2,1)} %copy-done.5, bf16[2,8,128,2048]{3,2,1,0:T(8,128)(2,1)} %get-tuple-element.7, f32[2,2048]{1,0:T(2,128)S(1)} %get-tuple-element.10, f32[2,2048]{1,0:T(2,128)S(1)} %get-tuple-element.11, f32[2048]{0:T(1024)S(1)} %copy-done.9, f32[2,8,128]{2,1,0:T(8,128)S(1)} %add_rsqrt_fusion, ...), kind=kOutput, calls=%fused_computation.14 | convolution fusion | flops 8621391872 | bytes 16826376 | tf_op jit(solution)/shard_map/dot_general | solution.py:528
  111.3 2.4 %fusion.16 = bf16[2,4,128,512]{3,2,1,0:T(8,128)(2,1)S(1)} fusion(bf16[2048,512]{1,0:T(8,128)(2,1)S(1)} %copy-done.8, bf16[2,8,128,2048]{3,2,1,0:T(8,128)(2,1)S(1)} %copy-done.1, f32[2,2048]{1,0:T(2,128)S(1)} %get-tuple-element.10, f32[2,2048]{1,0:T(2,128)S(1)} %get-tuple-element.11, f32[2048]{0:T(1024)S(1)} %copy-done.9, ...), kind=kOutput, calls=%fused_computation.19 | convolution fusion | flops 2177368064 | bytes 11583496 | tf_op jit(solution)/shard_map/dot_general | solution.py:530
  113.7 0.1 slice.52
  113.8 1.1 pad_maximum_fusion.q_ref
  114.9 0.8 copy-done.4
  115.7 1.5 copy.20
  117.2 0.7 reshape.110.bias_ref
  117.9 16.3 %shard_map.138 = bf16[2,8,64,512]{3,2,1,0:T(8,128)(2,1)} custom-call(f32[4,2,512]{2,1,0:T(2,128)} %reshape.110.bias_ref, f32[8]{0:T(128)} %far_ref.1, bf16[2,8,64,512]{3,2,1,0:T(8,128)(2,1)} %pad_maximum_fusion.q_ref, bf16[2,16,64,1024]{3,2,1,0:T(8,128)(2,1)} %bitcast.54, bf16[2,16,64,1024]{3,2,1,0:T(8,128)(2,1)} %bitcast.55, ...), custom_call_target="tpu_custom_call" | custom-call | flops 4294967296 | bytes 8388608 | tf_op jit(solution)/shard_map/pallas_call | solution.py:129
  134.3 1.2 slice.53
  135.5 0.9 slice.54
  136.4 0.1 pad_maximum_fusion.1
  136.5 0.1 copy.21
  136.6 2.3 %convolution_convert_fusion.parts_ref = bf16[4,256,2048]{2,1,0:T(8,128)(2,1)S(1)} fusion(bf16[4,256,512]{2,1,0:T(8,128)(2,1)S(1)} %bitcast.51, bf16[512,2048]{1,0:T(8,128)(2,1)S(1)} %copy-done), kind=kOutput, calls=%fused_computation.13 | convolution fusion | flops 2149580800 | bytes 7340032 | tf_op jit(solution)/shard_map/dot_general | solution.py:537
  139.0 28.1 %shard_map.139 = f32[256,2048]{1,0:T(8,128)S(1)} custom-call(bf16[4,256,2048]{2,1,0:T(8,128)(2,1)S(1)} %convolution_convert_fusion.parts_ref), custom_call_target="tpu_custom_call" | custom-call | tf_op jit(solution)/shard_map/pallas_call | solution.py:488
  167.1 1.3 add_convert_fusion
  (28 shorter events, 0.2 us)
Async XLA Ops:
  0.0 136.6 %copy-start = (bf16[512,2048]{1,0:T(8,128)(2,1)S(1)}, bf16[512,2048]{1,0:T(8,128)(2,1)}, u32[]{:S(2)}) copy-start(bf16[512,2048]{1,0:T(8,128)(2,1)} %param.25) | copy-start | bytes 6291460
  22.8 2.2 %copy-start.3 = (bf16[2048,512]{1,0:T(8,128)(2,1)S(1)}, bf16[2048,512]{1,0:T(8,128)(2,1)}, u32[]{:S(2)}) copy-start(bf16[2048,512]{1,0:T(8,128)(2,1)} %param.24) | copy-start | bytes 6291460
  22.9 2.5 %copy-start.6 = (bf16[2,64,2048]{2,1,0:T(8,128)(2,1)S(1)}, bf16[2,64,2048]{2,1,0:T(8,128)(2,1)}, u32[]{:S(2)}) copy-start(bf16[2,64,2048]{2,1,0:T(8,128)(2,1)} %param.15) | copy-start | bytes 1572868
  22.9 4.4 %copy-start.9 = (f32[2048]{0:T(1024)S(1)}, f32[2048]{0:T(1024)}, u32[]{:S(2)}) copy-start(f32[2048]{0:T(1024)} %param.21) | copy-start | bytes 24580
  25.4 1.9 %copy-start.5 = (bf16[2048,1024]{1,0:T(8,128)(2,1)}, bf16[2048,1024]{1,0:T(8,128)(2,1)S(1)}, u32[]{:S(2)}) copy-start(bf16[2048,1024]{1,0:T(8,128)(2,1)S(1)} %constant_dynamic-update-slice_fusion) | copy-start | bytes 12582916
  97.0 14.3 %copy-start.1 = (bf16[2,8,128,2048]{3,2,1,0:T(8,128)(2,1)S(1)}, bf16[2,8,128,2048]{3,2,1,0:T(8,128)(2,1)}, u32[]{:S(2)}) copy-start(bf16[2,8,128,2048]{3,2,1,0:T(8,128)(2,1)} %get-tuple-element.7) | copy-start | bytes 25165828
  97.0 14.3 %copy-start.8 = (bf16[2048,512]{1,0:T(8,128)(2,1)S(1)}, bf16[2048,512]{1,0:T(8,128)(2,1)}, u32[]{:S(2)}) copy-start(bf16[2048,512]{1,0:T(8,128)(2,1)} %param.22) | copy-start | bytes 6291460
  113.7 2.0 %copy-start.4 = (bf16[8,2,64,1024]{3,2,1,0:T(8,128)(2,1)S(1)}, bf16[8,2,64,1024]{3,2,1,0:T(8,128)(2,1)}, u32[]{:S(2)}) copy-start(bf16[8,2,64,1024]{3,2,1,0:T(8,128)(2,1)} %get-tuple-element.8) | copy-start | bytes 6291460
  113.7 3.5 %copy-start.7 = (f32[8,15,31]{2,0,1:T(8,128)S(1)}, f32[8,15,31]{2,0,1:T(8,128)}, u32[]{:S(2)}) copy-start(f32[8,15,31]{2,0,1:T(8,128)} %param.26) | copy-start | bytes 44644
  139.0 28.1 %copy-start.2 = (bf16[2,128,2048]{2,1,0:T(8,128)(2,1)S(1)}, bf16[2,128,2048]{2,1,0:T(8,128)(2,1)}, u32[]{:S(2)}) copy-start(bf16[2,128,2048]{2,1,0:T(8,128)(2,1)} %latent_ref.1) | copy-start | bytes 3145732

commit v3 on v1

--- a/solution.py
+++ b/solution.py
@@ -1,3 +1,5 @@
+import functools
+
 import jax
 import jax.numpy as jnp
 from jax import lax
@@ -72,9 +74,9 @@
                 table[h, 1, at_rows, :] = jnp.where(inside & inner, line, -jnp.inf)
 
     factor = HEAD_DIM ** (-0.5) * LOG2E
-    ck = ck_ref[0]
+    ck = ck_ref[...].reshape(-1, lanes)
     ctx_count = ck.shape[0]
-    cv = jnp.concatenate([cv_ref[0], jnp.ones((ctx_count, lanes), jnp.bfloat16)], axis=1)
+    cv = jnp.concatenate([cv_ref[...].reshape(-1, lanes), jnp.ones((ctx_count, lanes), jnp.bfloat16)], axis=1)
     ones = jnp.ones((nk, lanes), jnp.bfloat16)
     low = lax.broadcasted_iota(jnp.int32, (nq, lanes), 1) < HEAD_DIM
     contract = (((1,), (1,)), ((), ()))
@@ -115,7 +117,7 @@
 
 def attention(query, pair, ctx_pair, rel_bias, ctx_bias):
     samples, rows_dev, _, cols = query.shape
-    padded, ctx_count = pair.shape[1], ctx_pair.shape[1]
+    padded, ctx_count = pair.shape[1], ctx_pair.shape[0] * ctx_pair.shape[2]
     heads = cols // HEAD_DIM
     lanes = 2 * HEAD_DIM
     pairs = cols // lanes
@@ -123,7 +125,9 @@
     flat = jnp.pad(rel_bias, ((0, 0), (0, 1), (0, 1))).reshape(heads, -1)
     flat = jnp.pad(flat, ((0, 0), (0, nk - flat.shape[1]))).reshape(pairs, 2, nk)
     token = lambda at: pl.BlockSpec((1, padded, GRID_W, lanes), lambda p, s: (s, 0, 0, p + at))
-    far = lambda at: pl.BlockSpec((1, ctx_count, lanes), lambda p, s: (s, 0, p + at))
+    far = lambda at: pl.BlockSpec(
+        (ctx_pair.shape[0], 1, ctx_pair.shape[2], lanes), lambda p, s: (0, s, 0, p + at)
+    )
     own = pl.BlockSpec((1, rows_dev, GRID_W, lanes), lambda p, s: (s, 0, 0, p))
     scores = samples * heads * 4 * nq * (nk + ctx_count)
     return pl.pallas_call(
@@ -200,7 +204,7 @@
     padded_pair = extended(pair, (("sp", 1),), reach)
     half = WIN_COLS // 2
     rolled = jnp.roll(query, half, axis=2)
-    mixed = attention(rolled, padded_pair, ctx_pair, rel_bias, ctx_bias)
+    mixed = attention(rolled, padded_pair, ctx_pair[None], rel_bias, ctx_bias)
     attended = jnp.roll(mixed, -half, axis=2).reshape(samples, tokens_sp, local_cols)
     attended = attended.transpose(1, 0, 2)
     update = lax.psum_scatter(
@@ -216,9 +220,408 @@
     return result.astype(jnp.bfloat16)
 
 
+MESH = pl.DeviceIdType.MESH
+
+
+def entry_barrier(peers):
+    barrier = pltpu.get_barrier_semaphore()
+    for device, there in peers:
+        @pl.when(there)
+        def _():
+            pl.semaphore_signal(barrier, inc=1, device_id=device, device_id_type=MESH)
+    pl.semaphore_wait(barrier, sum(jnp.where(there, 1, 0) for _, there in peers))
+
+
+def front_kernel(
+    ada_ref, ws_ref, wc_ref, wg_ref, gain_ref, latent_ref, ctx_ref, wq_ref, wk_ref, wv_ref,
+    full_ref, q_ref, kv_ref, ckv_ref,
+    part, got, total, full, buf, wq, wkv, own_sem, s1, r1, s2, r2, s_ext, r_ext, s_ctx, r_ctx, r_sib,
+):
+    sp, tp = lax.axis_index("sp"), lax.axis_index("tp")
+    n_sp, n_tp = lax.axis_size("sp"), lax.axis_size("tp")
+    cols = part.shape[1]
+    over_sp = [lax.rem(sp + k, n_sp) for k in range(1, n_sp)]
+    over_tp = [lax.rem(tp + k, n_tp) for k in range(1, n_tp)]
+    always = sp >= 0
+    y, c = tp // 2, lax.rem(tp, 2)
+    z, x = sp // 2, lax.rem(sp, 2)
+    n_z = n_sp // 2
+    sib, across = y * 2 + 1 - c, (1 - y) * 2 + c
+    has_up, has_down = sp > 0, sp < n_sp - 1
+    direct = y * c + (1 - y) * (6 + c)
+    indirect = (1 - y) * c + y * (6 + c)
+    has_direct = ((y == 1) & has_up) | ((y == 0) & has_down)
+    has_indirect = ((y == 0) & has_up) | ((y == 1) & has_down)
+    toward = sp + 2 * y - 1
+    here, there = (sp, sib), (sp, across)
+    own_slot, across_slot = 2 + tp, 2 + across
+    x_peer = sp + 1 - 2 * x
+    beside, up, down = (x_peer, tp), (sp + 2, tp), (sp - 2, tp)
+    can_up, can_down = sp + 2 < n_sp, sp >= 2
+    half = buf.shape[1] // 2
+    part_of = pl.ds(pl.multiple_of(c * half, half), half)
+
+    locals_ = [
+        pltpu.make_async_copy(wq_ref, wq, own_sem.at[0]),
+        pltpu.make_async_copy(wk_ref, wkv.at[:, pl.ds(0, cols)], own_sem.at[1]),
+        pltpu.make_async_copy(wv_ref, wkv.at[:, pl.ds(cols, cols)], own_sem.at[2]),
+    ]
+    for copy in locals_:
+        copy.start()
+    own_copies = [
+        pltpu.make_async_copy(latent_ref.at[s], buf.at[s * 8 + own_slot], own_sem.at[3 + s])
+        for s in range(2)
+    ] + [
+        pltpu.make_async_copy(ctx_ref.at[s], buf.at[16 + sp, pl.ds(half * s, half)], own_sem.at[5 + s])
+        for s in range(2)
+    ]
+    for copy in own_copies:
+        copy.start()
+    entry_barrier([((p, tp), always) for p in over_sp] + [((sp, p), always) for p in over_tp])
+
+    early = []
+    mode = ["start"]
+
+    def send(cond, copy):
+        @pl.when(cond)
+        def _():
+            if mode[0] == "start":
+                copy.start()
+            else:
+                copy.wait_send()
+
+    def begin(cond, copy):
+        early.append((cond, copy))
+        send(cond, copy)
+
+    def arrived(cond, copy):
+        if mode[0] == "start":
+            @pl.when(cond)
+            def _():
+                copy.wait_recv()
+
+    def piece(flow, s, device, slot, own=False):
+        return pltpu.make_async_remote_copy(
+            src_ref=latent_ref.at[s] if own else buf.at[s * 8 + slot],
+            dst_ref=buf.at[s * 8 + slot],
+            send_sem=s_ext.at[flow, s], recv_sem=r_ext.at[flow, s],
+            device_id=device, device_id_type=MESH,
+        )
+
+    def block(at, way, device, own=False):
+        return pltpu.make_async_remote_copy(
+            src_ref=ctx_ref.at[c] if own else buf.at[16 + at, part_of],
+            dst_ref=buf.at[16 + at, part_of],
+            send_sem=s_ctx.at[at, way], recv_sem=(r_sib if way == 3 else r_ctx).at[at],
+            device_id=device, device_id_type=MESH,
+        )
+
+    def first(k, peer):
+        return pltpu.make_async_remote_copy(
+            src_ref=part, dst_ref=got.at[k], send_sem=s1.at[k], recv_sem=r1.at[k],
+            device_id=(peer, tp), device_id_type=MESH,
+        )
+
+    columns = pl.ds(pl.multiple_of(tp * cols, cols), cols)
+
+    def second(k, peer):
+        return pltpu.make_async_remote_copy(
+            src_ref=total, dst_ref=full.at[:, columns], send_sem=s2.at[k], recv_sem=r2.at[k],
+            device_id=(sp, peer), device_id_type=MESH,
+        )
+
+    for at, weight in enumerate((ws_ref, wc_ref, wg_ref)):
+        value = jnp.dot(ada_ref[...], weight[...], preferred_element_type=jnp.float32)
+        part[8 * at : 8 * at + 8, :] = value[:8]
+    firsts = [first(k, peer) for k, peer in enumerate(over_sp)]
+    for copy in firsts:
+        copy.start()
+    begin(always, piece(1, 0, there, own_slot, True))
+    begin(always, block(sp, 0, beside, True))
+    begin(can_up, block(sp, 1, up, True))
+    begin(can_down, block(sp, 2, down, True))
+    for s in range(2):
+        begin(has_indirect, piece(2, s, (toward, tp), direct, True))
+    for s in range(2):
+        begin(always, piece(0, s, here, own_slot, True))
+    value = part[...]
+    for k, copy in enumerate(firsts):
+        copy.wait()
+        value = value + got[k]
+    total[...] = value
+    seconds = [second(k, peer) for k, peer in enumerate(over_tp)]
+    for copy in seconds:
+        copy.start()
+    begin(always, piece(1, 1, there, own_slot, True))
+    full[:, columns] = value
+    for copy in locals_ + own_copies:
+        copy.wait()
+    for copy in seconds:
+        copy.wait()
+    full_ref[...] = full[...]
+
+    def neighbour_block():
+        arrived(always, block(x_peer, 0, beside))
+        send((c == 0) & can_up, block(x_peer, 1, up))
+        send((c == 0) & can_down, block(x_peer, 2, down))
+        send(always, block(x_peer, 3, here))
+
+    def relay(hop):
+        for e in range(2):
+            straight = (c == 0) | (x == e)
+            crossing = (c == 1) & (x == e)
+            low, high = sp - x - 2 * hop + e, sp - x + 2 * hop + e
+            for at, way, device, can, there_is in (
+                (lax.max(low, 0), 1, up, can_up, low >= 0),
+                (lax.min(high, n_sp - 1), 2, down, can_down, high < n_sp),
+            ):
+                arrived(there_is, block(at, way, device))
+                send(there_is & can & straight, block(at, way, device))
+                send(there_is & crossing, block(at, 0, beside))
+                send(there_is, block(at, 3, here))
+
+    def from_across(s):
+        arrived(always, piece(1, s, there, across_slot))
+        send(always, piece(3, s, here, across_slot))
+
+    def from_direct(s):
+        arrived(has_direct, piece(2, s, here, direct))
+        send(has_direct, piece(5, s, there, direct))
+        send(has_direct, piece(6, s, here, direct))
+
+    def from_indirect(s):
+        arrived(has_indirect, piece(5, s, there, indirect))
+        send(has_indirect, piece(7, s, here, indirect))
+
+    def sibling(flow, s, cond=always):
+        arrived(cond, piece(flow, s, here, own_slot))
+
+    def far_block(h, e):
+        zb = lax.rem(z + h, n_z)
+        at = 2 * zb + e
+        arrived(always, block(at, 3, here))
+
+    plan = []
+
+    def add(kind, s, events, at=0):
+        plan.append((kind, s, events, at))
+
+    add(0, 0, [])
+    add(0, 1, [])
+    add(1, 0, [neighbour_block, lambda: sibling(0, 0)])
+    add(1, 1, [lambda: sibling(0, 1)])
+    add(8, 0, [lambda: from_across(0)], sp)
+    add(2, 0, [lambda: from_direct(0)])
+    add(4, 0, [lambda: relay(1)] if n_z > 1 else [])
+    add(3, 0, [lambda: sibling(3, 0)])
+    add(5, 0, [lambda: sibling(6, 0, has_direct)])
+    add(8, 0, [lambda: arrived(always, block(x_peer, 3, here))], x_peer)
+    add(2, 1, [lambda: from_across(1)] + ([lambda: relay(2)] if n_z > 2 else []))
+    add(4, 1, [lambda: from_direct(1)])
+    add(3, 1, [lambda: sibling(3, 1)])
+    add(5, 1, [lambda: sibling(6, 1, has_direct)])
+    add(6, 0, [lambda: from_indirect(0)])
+    for hop in range(3, n_z):
+        plan[-1][2].append(functools.partial(relay, hop))
+    add(7, 0, [lambda: sibling(7, 0, has_indirect)])
+    for h in range(1, n_z):
+        for e in range(2):
+            add(8, 0, [functools.partial(far_block, h, e)], 2 * lax.rem(z + h, n_z) + e)
+    add(6, 1, [lambda: from_indirect(1)])
+    add(7, 1, [lambda: sibling(7, 1, has_indirect)])
+
+    slots = (own_slot, 2 + sib, across_slot, 2 + (1 - y) * 2 + 1 - c,
+             direct, direct + 1 - 2 * c, indirect, indirect + 1 - 2 * c)
+
+    def step(i, carry):
+        at = 0
+        row = 0
+        exists = 0
+        wants = 0
+        for k, (kind, s, events, ctx_at) in enumerate(plan):
+            on = jnp.where(i == k, 1, 0)
+            at = at + on * (16 + ctx_at if kind == 8 else s * 8 + slots[kind])
+            row = row + on * (2 if kind == 8 else s)
+            there_is = has_direct if kind in (4, 5) else has_indirect if kind in (6, 7) else always
+            exists = exists + on * jnp.where(there_is, 1, 0)
+            wants = wants + on * (1 if kind < 4 else 0)
+            if events:
+                @pl.when(i == k)
+                def _():
+                    for event in events:
+                        event()
+
+        @pl.when(exists == 1)
+        def _():
+            rows = buf[at].astype(jnp.float32)
+            inverse = lax.rsqrt(jnp.mean(rows * rows, axis=-1, keepdims=True) + EPSILON)
+            lift = gain_ref[...] * (1.0 + full[pl.ds(8 + row, 1), :])
+            hidden = (rows * inverse * lift + full[pl.ds(row, 1), :]).astype(jnp.bfloat16)
+            pair = jnp.dot(hidden, wkv[...], preferred_element_type=jnp.float32).astype(jnp.bfloat16)
+
+            @pl.when(at < 16)
+            def _():
+                kv_ref[lax.min(at, 15)] = pair
+
+            @pl.when(at >= 16)
+            def _():
+                ckv_ref[lax.max(at - 16, 0)] = pair
+
+            @pl.when(wants == 1)
+            def _():
+                place = lax.min(lax.max(at - 2 - 4 * row, 0), 7)
+                q_ref[place] = jnp.dot(
+                    hidden, wq[...], preferred_element_type=jnp.float32
+                ).astype(jnp.bfloat16)
+
+        @pl.when(exists == 0)
+        def _():
+            kv_ref[lax.min(at, 15)] = jnp.zeros(kv_ref.shape[1:], jnp.bfloat16)
+
+        return carry
+
+    lax.fori_loop(0, len(plan), step, 0)
+    mode[0] = "drain"
+    for cond, copy in early:
+        send(cond, copy)
+    for _, _, events, _ in plan:
+        for event in events:
+            event()
+
+
+def front(ada_rows, mods, gain, latent, context, w_query, w_key, w_value):
+    n_sp, n_tp = lax.axis_size("sp"), lax.axis_size("tp")
+    samples, tokens, width = latent.shape
+    cols = w_query.shape[1]
+    block = (24, cols)
+    ada_rows = jnp.pad(ada_rows, ((0, 16 - ada_rows.shape[0]), (0, 0)))
+    vmem, hbm = pl.BlockSpec(memory_space=pltpu.VMEM), pl.BlockSpec(memory_space=pl.ANY)
+    dma = pltpu.SemaphoreType.DMA
+    return pl.pallas_call(
+        front_kernel,
+        out_shape=(
+            jax.ShapeDtypeStruct((24, width), jnp.float32),
+            jax.ShapeDtypeStruct((samples * n_tp, tokens, cols), jnp.bfloat16),
+            jax.ShapeDtypeStruct((samples * 8, tokens, 2 * cols), jnp.bfloat16),
+            jax.ShapeDtypeStruct((n_sp, samples * context.shape[1], 2 * cols), jnp.bfloat16),
+        ),
+        in_specs=[vmem] * 7 + [hbm] * 3,
+        out_specs=[vmem] * 4,
+        scratch_shapes=[
+            pltpu.VMEM(block, jnp.float32),
+            pltpu.VMEM((n_sp - 1,) + block, jnp.float32),
+            pltpu.VMEM(block, jnp.float32),
+            pltpu.VMEM((24, width), jnp.float32),
+            pltpu.VMEM((16 + n_sp, tokens, width), jnp.bfloat16),
+            pltpu.VMEM((width, cols), jnp.bfloat16),
+            pltpu.VMEM((width, 2 * cols), jnp.bfloat16),
+            dma((7,)), dma((n_sp - 1,)), dma((n_sp - 1,)), dma((n_tp - 1,)), dma((n_tp - 1,)),
+            dma((8, 2)), dma((8, 2)), dma((n_sp, 4)), dma((n_sp,)), dma((n_sp,)),
+        ],
+        compiler_params=pltpu.CompilerParams(
+            collective_id=1, has_side_effects=True, vmem_limit_bytes=60 * 2**20
+        ),
+    )(ada_rows, *mods, gain[None, :], latent, context, w_query, w_key, w_value)
+
+
+def scatter_kernel(parts_ref, out_ref, got, summed, far, s1, r1, s2, r2):
+    sp, tp = lax.axis_index("sp"), lax.axis_index("tp")
+    y, c = tp // 2, lax.rem(tp, 2)
+    sib, across = y * 2 + 1 - c, (1 - y) * 2 + c
+    sib_across = (1 - y) * 2 + 1 - c
+    entry_barrier([((sp, sib), sp >= 0), ((sp, across), sp >= 0)])
+    chunks = far.shape[0]
+    rows = far.shape[1]
+
+    def near(k):
+        at = k % chunks
+        target = sib_across if k < chunks else sib
+        return pltpu.make_async_remote_copy(
+            src_ref=parts_ref.at[target, pl.ds(at * rows, rows)],
+            dst_ref=got.at[k],
+            send_sem=s1.at[k], recv_sem=r1.at[k],
+            device_id=(sp, sib), device_id_type=MESH,
+        )
+
+    def cross(k):
+        return pltpu.make_async_remote_copy(
+            src_ref=summed.at[k],
+            dst_ref=far.at[k],
+            send_sem=s2.at[k], recv_sem=r2.at[k],
+            device_id=(sp, across), device_id_type=MESH,
+        )
+
+    for k in range(2 * chunks):
+        near(k).start()
+    for k in range(chunks):
+        near(k).wait()
+        mine = parts_ref[across, k * rows : (k + 1) * rows, :].astype(jnp.float32)
+        summed[k] = (mine + got[k].astype(jnp.float32)).astype(jnp.bfloat16)
+        cross(k).start()
+    for k in range(chunks):
+        near(chunks + k).wait()
+        cross(k).wait()
+        mine = parts_ref[tp, k * rows : (k + 1) * rows, :].astype(jnp.float32)
+        mine = mine + got[chunks + k].astype(jnp.float32) + far[k].astype(jnp.float32)
+        out_ref[k * rows : (k + 1) * rows, :] = mine
+
+
+def scatter_sum(parts):
+    _, tokens, width = parts.shape
+    chunks = 4
+    rows = tokens // chunks
+    sems = [pltpu.SemaphoreType.DMA((2 * chunks,))] * 2 + [pltpu.SemaphoreType.DMA((chunks,))] * 2
+    return pl.pallas_call(
+        scatter_kernel,
+        out_shape=jax.ShapeDtypeStruct((tokens, width), jnp.float32),
+        in_specs=[pl.BlockSpec(memory_space=pltpu.VMEM)],
+        out_specs=pl.BlockSpec(memory_space=pltpu.VMEM),
+        scratch_shapes=[
+            pltpu.VMEM((2 * chunks, rows, width), jnp.bfloat16),
+            pltpu.VMEM((chunks, rows, width), jnp.bfloat16),
+            pltpu.VMEM((chunks, rows, width), jnp.bfloat16),
+        ]
+        + sems,
+        compiler_params=pltpu.CompilerParams(
+            collective_id=3, has_side_effects=True, vmem_limit_bytes=40 * 2**20
+        ),
+    )(parts)
+
+
+def on_four(
+    latent, context, cond, ctx_cond, w_shift, w_scale, w_gate, norm_gain,
+    w_query, w_key, w_value, w_out, rel_bias, ctx_bias,
+):
+    samples, tokens, width = latent.shape
+    n_sp, n_tp = lax.axis_size("sp"), lax.axis_size("tp")
+    rows_sp, local_cols = w_shift.shape
+    sp = lax.axis_index("sp")
+    ada = silu_rows(jnp.concatenate([cond, ctx_cond[None, :]], axis=0))
+    ada_rows = lax.dynamic_slice_in_dim(ada, sp * rows_sp, rows_sp, 1)
+    modulation, query, pair, ctx_pair = front(
+        ada_rows, (w_shift, w_scale, w_gate), norm_gain, latent, context, w_query, w_key, w_value
+    )
+    modulation = modulation.reshape(3, 8, width)
+    rows_dev = n_tp * tokens // GRID_W
+    query = query.reshape(samples, rows_dev, GRID_W, local_cols)
+    pair = pair.reshape(samples, 2 * rows_dev, GRID_W, 2 * local_cols)
+    ctx_pair = ctx_pair.reshape(n_sp, samples, -1, 2 * local_cols)
+    half = WIN_COLS // 2
+    rolled = jnp.roll(query, half, axis=2)
+    mixed = attention(rolled, pair, ctx_pair, rel_bias, ctx_bias)
+    attended = jnp.roll(mixed, -half, axis=2).reshape(samples, n_tp, tokens, local_cols)
+    attended = attended.transpose(1, 0, 2, 3).reshape(n_tp, samples * tokens, local_cols)
+    parts = jnp.dot(attended, w_out, preferred_element_type=jnp.float32).astype(jnp.bfloat16)
+    update = scatter_sum(parts).reshape(samples, tokens, width)
+    gate = modulation[2, :samples, None, :]
+    return (latent.astype(jnp.float32) + gate * update).astype(jnp.bfloat16)
+
+
 def solution(mesh):
+    shape = dict(mesh.shape)
+    quick = shape["tp"] == 4 and shape["sp"] == 8
     return jax.shard_map(
-        on_device,
+        on_four if quick else on_device,
         mesh=mesh,
         in_specs=(
             P(None, ("sp", "tp"), None),

time: 247 us -> 148 us (0.60)
  waiting for transfers between devices: 123 us -> 0 us
  Pallas kernels: 16.4 us -> 134 us
  blocking collectives: 44.2 us -> 0 us
  matrix products: 22.3 us -> 2.34 us
  between operations: 13.2 us -> 0.1 us
  other arithmetic: 12.2 us -> 3.19 us
  starting transfers between devices: 6.88 us -> 0 us
    pallas_call x0 -> x2, Pallas kernels: none -> 118 us  [the longest x1 86.2 us: front(): pl.pallas_call(front_kernel, out_shape=(jax.ShapeDtypeStruct((24, width),...]
    ppermute x2 -> x0, waiting for transfers between devices: 52 us -> none  [the longest x1 27.6 us: extended(): after = lax.ppermute(first, axis, down)]
    reduce_scatter x1 -> x0, waiting for transfers between devices: 44.6 us -> none  [on_device(): lax.psum_scatter(jnp.einsum('tsc,cd->tsd', attended, w_out, preferred_ele...]
    psum x1 -> x0, blocking collectives: 38.9 us -> none  [on_device(): summed = lax.psum(partial_value, 'sp')]
    all_gather x2 -> x0, waiting for transfers between devices: 26.5 us -> none  [the longest x1 26.5 us: on_device(): lax.all_gather(hidden, 'tp', axis=1, tiled=True)]
    dot_general x6 -> x1, matrix products: 22.3 us -> 2.34 us  [on_four(): jnp.dot(attended, w_out, preferred_element_type=jnp.float32)]
    ppermute x2 -> x0, starting transfers between devices: 6.8 us -> none  [the longest x1 5.52 us: extended(): before = lax.ppermute(last, axis, up)]
    all_gather x1 -> x0, blocking collectives: 5.31 us -> none  [on_device(): modulation = lax.all_gather(summed, 'tp', axis=2, tiled=True)]
  transfers between devices with their start and end apart: 5 -> 0, of which waited for: 4 -> 0; matrix products, arithmetic and copies ran while one was open for 10% -> 0% of each run, Pallas kernels for 0% -> 0%
where the time goes in v3:
time: 148 us; the launch traced here: 147 us
  Pallas kernels  134 us (91%)
  local copies, waits for them, and re-layouts  7.33 us (5%)
  other arithmetic  3.19 us (2%)
  matrix products  2.34 us (2%)
    pallas_call x1, Pallas kernels, front(): pl.pallas_call(front_kernel, out_shape=(jax.ShapeDtypeStruct((24, width),...  86.2 us
    pallas_call x1, Pallas kernels, scatter_sum(): pl.pallas_call(scatter_kernel, out_shape=jax.ShapeDtypeStruct((tokens, wi...  31.7 us
    pallas_call x1, Pallas kernels, attention(): pl.pallas_call(attention_kernel, grid=(pairs, samples), out_shape=jax.Sha...  16.4 us

profile of v3, /device:TPU:0, one launch (start us, length us, event | category | flops | bytes accessed | tf_op | source)
XLA Modules:
  0.0 147.2 jit_solution(4977797348018662880)
XLA Ops:
  0.0 0.0 copy-start
  0.0 0.8 broadcast_in_dim.6
  0.8 0.7 maximum_convert_fusion
  1.6 0.6 pad.8.ada_ref
  2.2 0.8 copy.17
  3.1 0.7 reshape.28.bias_ref
  3.8 86.2 %shard_map.136 = (f32[24,2048]{1,0:T(8,128)}, bf16[8,128,512]{2,1,0:T(8,128)(2,1)}, bf16[16,128,1024]{2,1,0:T(8,128)(2,1)}, bf16[8,128,1024]{2,1,0:T(8,128)(2,1)}) custom-call(bf16[16,256]{1,0:T(8,128)(2,1)} %pad.8.ada_ref, bf16[256,512]{1,0:T(8,128)(2,1)} %ws_ref.1, bf16[256,512]{1,0:T(8,128)(2,1)} %wc_ref.1, bf16[256,512]{1,0:T(8,128)(2,1)} %wg_ref.1, ...), custom_call_target="tpu_custom_call" | custom-call | tf_op jit(solution)/shard_map/pallas_call | solution.py:500
  90.0 0.8 slice_bitcast_fusion
  90.8 0.9 slice.25
  91.7 1.2 slice.26
  93.0 1.1 pad_maximum_fusion.q_ref
  94.0 16.4 %shard_map.137 = bf16[2,8,64,512]{3,2,1,0:T(8,128)(2,1)} custom-call(f32[4,2,512]{2,1,0:T(2,128)} %reshape.28.bias_ref, f32[8]{0:T(128)} %far_ref.1, bf16[2,8,64,512]{3,2,1,0:T(8,128)(2,1)} %pad_maximum_fusion.q_ref, bf16[2,16,64,1024]{3,2,1,0:T(8,128)(2,1)} %bitcast.23, bf16[2,16,64,1024]{3,2,1,0:T(8,128)(2,1)} %bitcast.24, ...), custom_call_target="tpu_custom_call" | custom-call | flops 4294967296 | bytes 8388608 | tf_op jit(solution)/shard_map/pallas_call | solution.py:133
  110.4 0.0 slice-start
  110.4 0.0 slice-start.1
  110.4 0.9 slice-done
  111.3 0.4 slice-done.1
  111.7 0.1 pad_maximum_fusion.1
  111.8 0.1 copy.16
  111.8 0.0 copy-done
  111.9 2.3 %convolution_convert_fusion.parts_ref = bf16[4,256,2048]{2,1,0:T(8,128)(2,1)S(1)} fusion(bf16[4,256,512]{2,1,0:T(8,128)(2,1)S(1)} %bitcast.20, bf16[512,2048]{1,0:T(8,128)(2,1)S(1)} %copy-done), kind=kOutput, calls=%fused_computation | convolution fusion | flops 2149580800 | bytes 7340032 | tf_op jit(solution)/shard_map/dot_general | solution.py:614
  114.2 0.0 copy-start.1
  114.2 31.7 %shard_map.138 = f32[256,2048]{1,0:T(8,128)S(1)} custom-call(bf16[4,256,2048]{2,1,0:T(8,128)(2,1)S(1)} %convolution_convert_fusion.parts_ref), custom_call_target="tpu_custom_call" | custom-call | tf_op jit(solution)/shard_map/pallas_call | solution.py:574
  145.9 0.0 copy-done.1
  145.9 1.3 add_convert_fusion
  (2 shorter events, 0.0 us)
Async XLA Ops:
  0.0 111.8 %copy-start = (bf16[512,2048]{1,0:T(8,128)(2,1)S(1)}, bf16[512,2048]{1,0:T(8,128)(2,1)}, u32[]{:S(2)}) copy-start(bf16[512,2048]{1,0:T(8,128)(2,1)} %param.25) | copy-start | bytes 6291460
  110.4 0.9 slice-start
  110.4 1.3 slice-start.1
  114.2 31.7 %copy-start.1 = (bf16[2,128,2048]{2,1,0:T(8,128)(2,1)S(1)}, bf16[2,128,2048]{2,1,0:T(8,128)(2,1)}, u32[]{:S(2)}) copy-start(bf16[2,128,2048]{2,1,0:T(8,128)(2,1)} %latent_ref.1) | copy-start | bytes 3145732

commit v4 on v3

--- a/solution.py
+++ b/solution.py
@@ -80,8 +80,14 @@
     ones = jnp.ones((nk, lanes), jnp.bfloat16)
     low = lax.broadcasted_iota(jnp.int32, (nq, lanes), 1) < HEAD_DIM
     contract = (((1,), (1,)), ((), ()))
+    every = q_ref[0].astype(jnp.float32)
+    outs = []
     for block in range(GRID_W // WIN_COLS):
-        q = q_ref[0, :, WIN_COLS * block : WIN_COLS * (block + 1), :].reshape(nq, lanes)
+        if block == 0:
+            q = jnp.concatenate([every[:, GRID_W - half :], every[:, :half]], axis=1)
+        else:
+            q = every[:, WIN_COLS * block - half : WIN_COLS * (block + 1) - half]
+        q = q.astype(jnp.bfloat16).reshape(nq, lanes)
 
         def keys(ref):
             if block == 0:
@@ -109,10 +115,9 @@
                 far, cv, preferred_element_type=jnp.float32
             )
             halves.append(got[:, :lanes] / got[:, lanes:])
-        got = jnp.where(low, halves[0], halves[1]).astype(jnp.bfloat16)
-        out_ref[0, :, WIN_COLS * block : WIN_COLS * (block + 1), :] = got.reshape(
-            rows_dev, WIN_COLS, lanes
-        )
+        outs.append(jnp.where(low, halves[0], halves[1]).reshape(rows_dev, WIN_COLS, lanes))
+    outs = [outs[0][:, half:]] + outs[1:] + [outs[0][:, :half]]
+    out_ref[0] = jnp.concatenate(outs, axis=1).astype(jnp.bfloat16)
 
 
 def attention(query, pair, ctx_pair, rel_bias, ctx_bias):
@@ -202,10 +207,8 @@
     query = triple[..., :local_cols].reshape(samples, rows_dev, GRID_W, local_cols)
     pair = triple[..., local_cols:].reshape(samples, rows_dev, GRID_W, 2 * local_cols)
     padded_pair = extended(pair, (("sp", 1),), reach)
-    half = WIN_COLS // 2
-    rolled = jnp.roll(query, half, axis=2)
-    mixed = attention(rolled, padded_pair, ctx_pair[None], rel_bias, ctx_bias)
-    attended = jnp.roll(mixed, -half, axis=2).reshape(samples, tokens_sp, local_cols)
+    mixed = attention(query, padded_pair, ctx_pair[None], rel_bias, ctx_bias)
+    attended = mixed.reshape(samples, tokens_sp, local_cols)
     attended = attended.transpose(1, 0, 2)
     update = lax.psum_scatter(
         jnp.einsum("tsc,cd->tsd", attended, w_out, preferred_element_type=jnp.float32).astype(
@@ -269,7 +272,7 @@
     for copy in locals_:
         copy.start()
     own_copies = [
-        pltpu.make_async_copy(latent_ref.at[s], buf.at[s * 8 + own_slot], own_sem.at[3 + s])
+        pltpu.make_async_copy(latent_ref.at[s], buf.at[2 * own_slot + s], own_sem.at[3 + s])
         for s in range(2)
     ] + [
         pltpu.make_async_copy(ctx_ref.at[s], buf.at[16 + sp, pl.ds(half * s, half)], own_sem.at[5 + s])
@@ -302,8 +305,8 @@
 
     def piece(flow, s, device, slot, own=False):
         return pltpu.make_async_remote_copy(
-            src_ref=latent_ref.at[s] if own else buf.at[s * 8 + slot],
-            dst_ref=buf.at[s * 8 + slot],
+            src_ref=latent_ref.at[s] if own else buf.at[2 * slot + s],
+            dst_ref=buf.at[2 * slot + s],
             send_sem=s_ext.at[flow, s], recv_sem=r_ext.at[flow, s],
             device_id=device, device_id_type=MESH,
         )
@@ -406,29 +409,21 @@
     def add(kind, s, events, at=0):
         plan.append((kind, s, events, at))
 
+    both = lambda flow, cond=always: [functools.partial(sibling, flow, e, cond) for e in range(2)]
     add(0, 0, [])
-    add(0, 1, [])
-    add(1, 0, [neighbour_block, lambda: sibling(0, 0)])
-    add(1, 1, [lambda: sibling(0, 1)])
-    add(8, 0, [lambda: from_across(0)], sp)
-    add(2, 0, [lambda: from_direct(0)])
-    add(4, 0, [lambda: relay(1)] if n_z > 1 else [])
-    add(3, 0, [lambda: sibling(3, 0)])
-    add(5, 0, [lambda: sibling(6, 0, has_direct)])
-    add(8, 0, [lambda: arrived(always, block(x_peer, 3, here))], x_peer)
-    add(2, 1, [lambda: from_across(1)] + ([lambda: relay(2)] if n_z > 2 else []))
-    add(4, 1, [lambda: from_direct(1)])
-    add(3, 1, [lambda: sibling(3, 1)])
-    add(5, 1, [lambda: sibling(6, 1, has_direct)])
-    add(6, 0, [lambda: from_indirect(0)])
-    for hop in range(3, n_z):
-        plan[-1][2].append(functools.partial(relay, hop))
-    add(7, 0, [lambda: sibling(7, 0, has_indirect)])
+    add(1, 0, [neighbour_block] + both(0))
+    from_peer = lambda: arrived(always, block(x_peer, 3, here))
+    add(8, 0, [functools.partial(from_across, 0), functools.partial(from_direct, 0), from_peer], 2 * z)
+    add(2, 0, [functools.partial(relay, 1), functools.partial(from_across, 1)])
+    add(4, 0, [functools.partial(from_direct, 1)])
+    add(3, 0, [functools.partial(relay, 2)] + both(3))
+    add(5, 0, both(6, has_direct))
+    hops = [functools.partial(relay, hop) for hop in range(3, n_z)]
     for h in range(1, n_z):
-        for e in range(2):
-            add(8, 0, [functools.partial(far_block, h, e)], 2 * lax.rem(z + h, n_z) + e)
-    add(6, 1, [lambda: from_indirect(1)])
-    add(7, 1, [lambda: sibling(7, 1, has_indirect)])
+        waits = [functools.partial(far_block, h, e) for e in range(2)]
+        add(8, 0, (hops + [functools.partial(from_indirect, 0)] if h == 1 else []) + waits, 2 * lax.rem(z + h, n_z))
+    add(6, 0, [functools.partial(from_indirect, 1)])
+    add(7, 0, both(7, has_indirect))
 
     slots = (own_slot, 2 + sib, across_slot, 2 + (1 - y) * 2 + 1 - c,
              direct, direct + 1 - 2 * c, indirect, indirect + 1 - 2 * c)
@@ -440,8 +435,8 @@
         wants = 0
         for k, (kind, s, events, ctx_at) in enumerate(plan):
             on = jnp.where(i == k, 1, 0)
-            at = at + on * (16 + ctx_at if kind == 8 else s * 8 + slots[kind])
-            row = row + on * (2 if kind == 8 else s)
+            at = at + on * (16 + ctx_at if kind == 8 else 2 * slots[kind])
+            row = row + on * (1 if kind == 8 else 0)
             there_is = has_direct if kind in (4, 5) else has_indirect if kind in (6, 7) else always
             exists = exists + on * jnp.where(there_is, 1, 0)
             wants = wants + on * (1 if kind < 4 else 0)
@@ -453,30 +448,40 @@
 
         @pl.when(exists == 1)
         def _():
-            rows = buf[at].astype(jnp.float32)
-            inverse = lax.rsqrt(jnp.mean(rows * rows, axis=-1, keepdims=True) + EPSILON)
-            lift = gain_ref[...] * (1.0 + full[pl.ds(8 + row, 1), :])
-            hidden = (rows * inverse * lift + full[pl.ds(row, 1), :]).astype(jnp.bfloat16)
+            hidden = []
+            for e in range(2):
+                rows = buf[at + e].astype(jnp.float32)
+                inverse = lax.rsqrt(jnp.mean(rows * rows, axis=-1, keepdims=True) + EPSILON)
+                which = e + row * (2 - e)
+                lift = gain_ref[...] * (1.0 + full[pl.ds(8 + which, 1), :])
+                rows = rows * inverse * lift + full[pl.ds(which, 1), :]
+                hidden.append(rows.astype(jnp.bfloat16))
+            hidden = jnp.concatenate(hidden, axis=0)
+            count = hidden.shape[0] // 2
             pair = jnp.dot(hidden, wkv[...], preferred_element_type=jnp.float32).astype(jnp.bfloat16)
 
             @pl.when(at < 16)
             def _():
-                kv_ref[lax.min(at, 15)] = pair
+                for e in range(2):
+                    kv_ref[lax.div(lax.min(at, 14), 2) + 8 * e] = pair[e * count : (e + 1) * count]
 
             @pl.when(at >= 16)
             def _():
-                ckv_ref[lax.max(at - 16, 0)] = pair
+                for e in range(2):
+                    ckv_ref[lax.max(at - 16, 0) + e] = pair[e * count : (e + 1) * count]
 
             @pl.when(wants == 1)
             def _():
-                place = lax.min(lax.max(at - 2 - 4 * row, 0), 7)
-                q_ref[place] = jnp.dot(
-                    hidden, wq[...], preferred_element_type=jnp.float32
-                ).astype(jnp.bfloat16)
+                query = jnp.dot(hidden, wq[...], preferred_element_type=jnp.float32)
+                query = query.astype(jnp.bfloat16)
+                for e in range(2):
+                    place = lax.div(lax.min(lax.max(at - 4, 0), 6), 2) + 4 * e
+                    q_ref[place] = query[e * count : (e + 1) * count]
 
         @pl.when(exists == 0)
         def _():
-            kv_ref[lax.min(at, 15)] = jnp.zeros(kv_ref.shape[1:], jnp.bfloat16)
+            for e in range(2):
+                kv_ref[lax.div(lax.min(at, 14), 2) + 8 * e] = jnp.zeros(kv_ref.shape[1:], jnp.bfloat16)
 
         return carry
 
@@ -606,10 +611,8 @@
     query = query.reshape(samples, rows_dev, GRID_W, local_cols)
     pair = pair.reshape(samples, 2 * rows_dev, GRID_W, 2 * local_cols)
     ctx_pair = ctx_pair.reshape(n_sp, samples, -1, 2 * local_cols)
-    half = WIN_COLS // 2
-    rolled = jnp.roll(query, half, axis=2)
-    mixed = attention(rolled, pair, ctx_pair, rel_bias, ctx_bias)
-    attended = jnp.roll(mixed, -half, axis=2).reshape(samples, n_tp, tokens, local_cols)
+    mixed = attention(query, pair, ctx_pair, rel_bias, ctx_bias)
+    attended = mixed.reshape(samples, n_tp, tokens, local_cols)
     attended = attended.transpose(1, 0, 2, 3).reshape(n_tp, samples * tokens, local_cols)
     parts = jnp.dot(attended, w_out, preferred_element_type=jnp.float32).astype(jnp.bfloat16)
     update = scatter_sum(parts).reshape(samples, tokens, width)

time: 148 us -> 140 us (0.946)
  Pallas kernels: 134 us -> 130 us
  local copies, waits for them, and re-layouts: 7.33 us -> 5.18 us
    slice x6 -> x0, local copies, waits for them, and re-layouts: 3.41 us -> none  [the longest x2 2.16 us: on_four(): rolled = jnp.roll(query, half, axis=2)]
    pallas_call x1, Pallas kernels: 31.7 us -> 29 us  [scatter_sum(): pl.pallas_call(scatter_kernel, out_shape=jax.ShapeDtypeStruct((tokens, wi...]
where the time goes in v4:
time: 140 us
  Pallas kernels  130 us (93%)
  local copies, waits for them, and re-layouts  5.18 us (4%)
  matrix products  2.34 us (2%)
  other arithmetic  2.01 us (1%)
    pallas_call x1, Pallas kernels, front(): pl.pallas_call(front_kernel, out_shape=(jax.ShapeDtypeStruct((24, width),...  84.8 us
    pallas_call x1, Pallas kernels, scatter_sum(): pl.pallas_call(scatter_kernel, out_shape=jax.ShapeDtypeStruct((tokens, wi...  29 us
    pallas_call x1, Pallas kernels, attention(): pl.pallas_call(attention_kernel, grid=(pairs, samples), out_shape=jax.Sha...  16.4 us

profile of v4, /device:TPU:0, one launch (start us, length us, event | category | flops | bytes accessed | tf_op | source)
XLA Modules:
  0.0 139.8 jit_solution(16422913198282073390)
XLA Ops:
  0.0 0.0 copy-start
  0.0 0.8 broadcast_in_dim.6
  0.8 0.7 maximum_convert_fusion
  1.6 0.6 pad.8.ada_ref
  2.2 0.8 copy.17
  3.1 0.7 reshape.28.bias_ref
  3.8 84.8 %shard_map.136 = (f32[24,2048]{1,0:T(8,128)}, bf16[8,128,512]{2,1,0:T(8,128)(2,1)}, bf16[16,128,1024]{2,1,0:T(8,128)(2,1)}, bf16[8,128,1024]{2,1,0:T(8,128)(2,1)}) custom-call(bf16[16,256]{1,0:T(8,128)(2,1)} %pad.8.ada_ref, bf16[256,512]{1,0:T(8,128)(2,1)} %ws_ref.1, bf16[256,512]{1,0:T(8,128)(2,1)} %wc_ref.1, bf16[256,512]{1,0:T(8,128)(2,1)} %wg_ref.1, ...), custom_call_target="tpu_custom_call" | custom-call | tf_op jit(solution)/shard_map/pallas_call | solution.py:505
  88.5 0.8 slice_bitcast_fusion
  89.4 16.4 %shard_map.137 = bf16[2,8,64,512]{3,2,1,0:T(8,128)(2,1)} custom-call(f32[4,2,512]{2,1,0:T(2,128)} %reshape.28.bias_ref, f32[8]{0:T(128)} %far_ref.1, bf16[2,8,64,512]{3,2,1,0:T(8,128)(2,1)} %bitcast.25, bf16[2,16,64,1024]{3,2,1,0:T(8,128)(2,1)} %bitcast.21, bf16[2,16,64,1024]{3,2,1,0:T(8,128)(2,1)} %bitcast.22, bf16[8,2,64,1024]{3,2,1,0:T(8,128)(2,1)} %bitcast.23, ...), custom_call_target="tpu_custom_call" | custom-call | flops 4294967296 | bytes 8388608 | tf_op jit(solution)/shard_map/pallas_call | solution.py:138
  105.8 1.3 copy.16
  107.1 0.0 copy-done
  107.1 2.3 %convolution_convert_fusion.parts_ref = bf16[4,256,2048]{2,1,0:T(8,128)(2,1)S(1)} fusion(bf16[4,256,512]{2,1,0:T(8,128)(2,1)S(1)} %bitcast.18, bf16[512,2048]{1,0:T(8,128)(2,1)S(1)} %copy-done), kind=kOutput, calls=%fused_computation | convolution fusion | flops 2149580800 | bytes 7340032 | tf_op jit(solution)/shard_map/dot_general | solution.py:617
  109.5 0.0 copy-start.1
  109.5 29.0 %shard_map.138 = f32[256,2048]{1,0:T(8,128)S(1)} custom-call(bf16[4,256,2048]{2,1,0:T(8,128)(2,1)S(1)} %convolution_convert_fusion.parts_ref), custom_call_target="tpu_custom_call" | custom-call | tf_op jit(solution)/shard_map/pallas_call | solution.py:579
  138.5 0.0 copy-done.1
  138.5 1.3 add_convert_fusion
  (2 shorter events, 0.0 us)
Async XLA Ops:
  0.0 107.1 %copy-start = (bf16[512,2048]{1,0:T(8,128)(2,1)S(1)}, bf16[512,2048]{1,0:T(8,128)(2,1)}, u32[]{:S(2)}) copy-start(bf16[512,2048]{1,0:T(8,128)(2,1)} %param.25) | copy-start | bytes 6291460
  109.5 29.0 %copy-start.1 = (bf16[2,128,2048]{2,1,0:T(8,128)(2,1)S(1)}, bf16[2,128,2048]{2,1,0:T(8,128)(2,1)}, u32[]{:S(2)}) copy-start(bf16[2,128,2048]{2,1,0:T(8,128)(2,1)} %latent_ref.1) | copy-start | bytes 3145732
